TPU v7x, 128 devices: a whole 4x4x4 slice. The times are simulated.
128 devices in a mesh: sp: 32 (over z, y, core), tp: 4 (over x).
Axes of the slice: x: 4, y: 4, z: 4, core: 2. Of those that a mesh axis runs over, the one named last changes fastest.
Arguments:
- conv_value: bfloat16 [16384, 2048], P('sp', 'tp'), may hold values from -6 to 6
- conv_gate: bfloat16 [16384, 2048], P('sp', 'tp'), may hold values from -6 to 6
- conv_taps: float32 [31, 2048], P(None, 'tp'), as said below
- channel_gain: float32 [2048], P('tp'), may hold values from 0.1 to 1.9
- point_weight: bfloat16 [2048, 2048], replicated, may hold values from -0.125 to 0.125
- residual_in: bfloat16 [16384, 2048], P(('sp', 'tp')), may hold values from -3 to 3
- first_gain: float32 [2048], replicated, may hold values from 0.1 to 1.9
- second_gain: float32 [2048], replicated, may hold values from 0.1 to 1.9
- routes: int32 [16384, 2], P(('sp', 'tp')), may hold values from 0 to 127, all different within a row; in each aligned block of 128 rows (0 to 127, 128 to 255, ...) at most 4 rows name the same one
- route_score: float32 [16384, 2], P(('sp', 'tp')), may hold values from 0.1 to 1
- expert_gate: bfloat16 [128, 2048, 1024], P(('sp', 'tp')), may hold values from -0.125 to 0.125
- expert_up: bfloat16 [128, 2048, 1024], P(('sp', 'tp')), may hold values from -0.125 to 0.125
- expert_down: bfloat16 [128, 1024, 2048], P(('sp', 'tp')), may hold values from -0.1875 to 0.1875
Outputs:
- layer_out: bfloat16 [16384, 2048], P(('sp', 'tp'))
Inputs may be any that keep to these rules, and one draw needn't show every extreme that they name: `routes`: among the 128 rows of one device (aligned blocks of rows), no expert is named more than 4 times, a bound that some block reaches; a row names 2 different experts. conv_taps have independent entries, with scales that differ from channel to channel.
All inputs are finite; a program needn't handle non-finite values.
Results may differ from a plain program's by a relative error of at most 0.013.
Values may be sent and summed in bfloat16 or wider, within the bound.
A program may use at most 128 MiB of HBM per device.

v0:
```python
import jax
import jax.numpy as jnp
from jax import lax
from jax.sharding import PartitionSpec as P

residual_scale = 8.0**0.25


def from_behind(block, axis, distance):
    devices = range(lax.axis_size(axis))
    route = [(i - distance, i) for i in devices if i - distance in devices]
    return lax.ppermute(block, axis, route)


def token_norm(values, gain):
    middle = jnp.mean(values, axis=-1, keepdims=True)
    centred = values - middle
    spread = jnp.mean(centred * centred, axis=-1, keepdims=True)
    return centred * lax.rsqrt(spread + 1e-05) * gain


def per_device(
    conv_value,
    conv_gate,
    conv_taps,
    channel_gain,
    point_weight,
    residual_in,
    first_gain,
    second_gain,
    routes,
    route_score,
    expert_gate,
    expert_up,
    expert_down,
):
    edge = conv_taps.shape[0] - 1
    local_width = conv_value.shape[1]
    rim_value, rim_gate = from_behind((conv_value[-edge:], conv_gate[-edge:]), "sp", 1)
    ext_value = jnp.concatenate([rim_value, conv_value], axis=0)
    ext_gate = jnp.concatenate([rim_gate, conv_gate], axis=0)
    glu = ext_value.astype(jnp.float32) * jax.nn.sigmoid(ext_gate.astype(jnp.float32))
    conv = lax.conv_general_dilated(
        glu[None],
        conv_taps[:, None, :],
        (1,),
        [(0, 0)],
        dimension_numbers=("NWC", "WIO", "NWC"),
        feature_group_count=local_width,
    )[0]
    width = local_width * lax.axis_size("tp")
    sums, squares = lax.psum((jnp.sum(conv, axis=1), jnp.sum(conv * conv, axis=1)), "tp")
    middle = sums / width
    spread = squares / width - middle * middle
    normed = (conv - middle[:, None]) * lax.rsqrt(spread + 1e-05)[:, None] * channel_gain
    act = (normed * jax.nn.sigmoid(normed)).astype(jnp.bfloat16)
    rows = act.shape[0] // lax.axis_size("tp")
    owned = lax.all_to_all(act, "tp", split_axis=0, concat_axis=1, tiled=True)
    mix = jnp.dot(owned, point_weight, preferred_element_type=jnp.float32)
    first = token_norm(residual_scale * residual_in.astype(jnp.float32) + mix, first_gain).astype(
        jnp.bfloat16
    )
    top = routes.shape[1]
    model_width = first.shape[1]
    experts = lax.axis_size("sp") * lax.axis_size("tp")
    capacity = max(2, 2 * rows * top // experts)
    flat_e = routes.reshape(-1)
    onehot = (flat_e[:, None] == jnp.arange(experts, dtype=jnp.int32)[None, :]).astype(jnp.int32)
    before = jnp.sum((jnp.cumsum(onehot, axis=0) - onehot) * onehot, axis=1)
    slot = flat_e * capacity + before
    source = jnp.repeat(first, top, axis=0)
    outgoing = (
        jnp.zeros((experts * capacity, model_width), jnp.bfloat16)
        .at[slot]
        .set(source)
        .reshape(experts, capacity, model_width)
    )
    received = lax.all_to_all(outgoing, ("sp", "tp"), split_axis=0, concat_axis=0, tiled=True)
    shape = received.shape
    flat = received.reshape(-1, model_width)
    gate = jnp.dot(flat, expert_gate[0], preferred_element_type=jnp.float32)
    upper = jnp.dot(flat, expert_up[0], preferred_element_type=jnp.float32)
    hidden = (jax.nn.silu(gate) * upper).astype(jnp.bfloat16)
    answer = jnp.dot(hidden, expert_down[0], preferred_element_type=jnp.float32).astype(
        jnp.bfloat16
    )
    returned = lax.all_to_all(
        answer.reshape(shape), ("sp", "tp"), split_axis=0, concat_axis=0, tiled=True
    )
    per_assign = returned.reshape(experts * capacity, model_width)[slot]
    share = route_score / jnp.sum(route_score, axis=1, keepdims=True)
    moe = jnp.sum(
        share[:, :, None] * per_assign.reshape(rows, top, model_width).astype(jnp.float32), axis=1
    )
    return token_norm(residual_scale * first.astype(jnp.float32) + moe, second_gain).astype(
        jnp.bfloat16
    )


def solution(mesh):
    in_specs = (
        P("sp", "tp"),
        P("sp", "tp"),
        P(None, "tp"),
        P("tp"),
        P(),
        P(("sp", "tp"), None),
        P(),
        P(),
        P(("sp", "tp"), None),
        P(("sp", "tp"), None),
        P(("sp", "tp"), None, None),
        P(("sp", "tp"), None, None),
        P(("sp", "tp"), None, None),
    )
    out_specs = P(("sp", "tp"), None)
    return jax.shard_map(
        per_device, mesh=mesh, in_specs=in_specs, out_specs=out_specs, check_vma=False
    )
```

profile of v0, /device:TPU:1, one launch (start us, length us, event | category | flops | bytes accessed | tf_op | source)
XLA Modules:
  0.0 163.4 jit_solution(13603696976365561606)
XLA Ops:
  0.0 0.8 slice.12
  0.8 4.6 %collective-permute-start = (bf16[30,512]{1,0:T(8,128)(2,1)S(1)}, bf16[30,512]{1,0:T(8,128)(2,1)S(1)}, u32[]{:S(2)}, u32[]{:S(2)}) collective-permute-start(bf16[30,512]{1,0:T(8,128)(2,1)S(1)} %slice.12), channel_id=1, source_target_pairs={{0,4},{4,8},{8,12},{12,16},{16,20},{20,24},{24,28},{28,32},{32,36}... | collective-permute-start | bytes 92168 | tf_op jit(solution)/shard_map/ppermute | solution.py:12
  5.4 0.8 slice.13
  6.2 1.9 %collective-permute-start.1 = (bf16[30,512]{1,0:T(8,128)(2,1)S(1)}, bf16[30,512]{1,0:T(8,128)(2,1)S(1)}, u32[]{:S(2)}, u32[]{:S(2)}) collective-permute-start(bf16[30,512]{1,0:T(8,128)(2,1)S(1)} %slice.13), channel_id=1, source_target_pairs={{0,4},{4,8},{8,12},{12,16},{16,20},{20,24},{24,28},{28,32},{32,36}... | collective-permute-start | bytes 92168 | tf_op jit(solution)/shard_map/ppermute | solution.py:12
  8.1 0.8 copy.24
  8.9 0.1 eq.29
  9.0 0.1 copy.26
  9.1 0.2 fusion.26
  9.4 0.7 broadcast_add_fusion
  10.1 1.6 divide_multiply_fusion
  11.8 0.3 reshape.196
  12.1 0.3 copy.17
  12.5 2.4 %fusion.36 = (f32[8,68,512]{2,0,1:T(8,128)S(1)}, f32[8,68,512]{2,0,1:T(8,128)S(1)}) fusion(f32[31,1,512]{2,0,1:T(8,128)S(1)} %bitcast.54, bf16[1,7,30,512]{3,1,2,0:T(8,128)(2,1)S(1)} %slice.21, bf16[1,8,68,512]{3,1,2,0:T(8,128)(2,1)S(1)} %copy.17, pred[8,68]{0,1:T(8,128)(4,1)S(1)} %copy-done.9), kind=kOutput, calls=%fused_computation.58 | convolution fusion | flops 20234240 | bytes 3064352 | tf_op jit(solution)/shard_map/conv_general_dilated | solution.py:43
  14.9 0.6 copy.19
  15.6 0.1 reshape.200
  15.7 0.7 copy.21
  16.5 0.2 slice_reduce_fusion.1
  16.7 0.3 copy.20
  17.1 8.6 %all-reduce = (f32[512]{0:T(512)S(1)}, f32[512]{0:T(512)S(1)}) all-reduce(f32[512]{0:T(512)S(1)} %get-tuple-element.15, f32[512]{0:T(512)S(1)} %get-tuple-element.7), channel_id=1, replica_groups=mesh['sp'=32,'tp'=4] {'tp'}, use_global_device_ids=true, to_apply=%region_3.0 | all-reduce | flops 1024 | bytes 8192 | tf_op jit(solution)/shard_map/psum | solution.py:52
  25.7 1.2 multiply_convert_fusion.3
  26.9 3.5 %all-to-all-start = ((bf16[4,128,512]{1,2,0:T(8,128)(2,1)}), bf16[4,128,512]{1,2,0:T(8,128)(2,1)S(1)}, u32[]{:S(2)}, u32[]{:S(2)}) async-start(bf16[4,128,512]{1,2,0:T(8,128)(2,1)} %multiply_convert_fusion.3), calls=%async_computation | async-start | bytes 1048576 | tf_op jit(solution)/shard_map/all_to_all | solution.py:58
  30.4 0.1 eq.25
  30.6 0.1 copy.23
  30.7 0.1 mul.138
  30.8 0.2 fusion.28
  31.0 6.3 %all-to-all-done = bf16[4,128,512]{1,2,0:T(8,128)(2,1)S(1)} async-done(((bf16[4,128,512]{1,2,0:T(8,128)(2,1)}), bf16[4,128,512]{1,2,0:T(8,128)(2,1)S(1)}, u32[]{:S(2)}, u32[]{:S(2)}) %all-to-all-start) | async-done | bytes 524320 | tf_op jit(solution)/shard_map/all_to_all | solution.py:58
  37.3 4.8 %fusion.37 = (f32[128]{0:T(128)S(1)}, f32[128,2048]{1,0:T(8,128)S(1)}) fusion(bf16[128,2048]{0,1:T(8,128)(2,1)S(1)} %bitcast.56, bf16[2048,2048]{1,0:T(8,128)(2,1)} %param.17, bf16[128,2048]{1,0:T(8,128)(2,1)S(1)} %copy-done.2), kind=kOutput, calls=%fused_computation.59 | convolution fusion | flops 1074790272 | bytes 10486272 | tf_op jit(solution)/shard_map/dot_general | solution.py:59
  42.0 0.3 multiply_reduce_fusion.2
  42.3 0.2 multiply_convert_fusion.2
  42.5 0.6 broadcast_in_dim.8
  43.2 1.2 reshape.220
  44.4 3.7 %scatter_custom_fusion = bf16[512,2048]{1,0:T(8,128)(2,1)S(1)} fusion(s32[256]{0:T(256)S(1)} %bitcast.65, bf16[256,2048]{1,0:T(8,128)(2,1)} %reshape.220, bf16[]{:T(256)} %constant.32.clone.1), kind=kCustom, calls=%fused_computation.23 | custom fusion | bytes 2097664 | tf_op jit(solution)/shard_map/scatter | solution.py:75
  48.1 2.2 %reshape.190 = bf16[128,4,2048]{2,1,0:T(4,128)(2,1)} reshape(bf16[512,2048]{1,0:T(8,128)(2,1)S(1)} %scatter_custom_fusion) | data formatting | bytes 4194304 | tf_op jit(solution)/shard_map/reshape | solution.py:76
  50.3 42.3 %all_to_all.26 = bf16[128,4,2048]{2,1,0:T(4,128)(2,1)S(1)} all-to-all(bf16[128,4,2048]{2,1,0:T(4,128)(2,1)} %reshape.190), channel_id=1, replica_groups=mesh['sp'=32,'tp'=4] {'sp','tp'}, dimensions={0} | all-to-all | bytes 4194304 | tf_op jit(solution)/shard_map/all_to_all | solution.py:78
  92.6 2.0 %reshape.191 = bf16[512,2048]{1,0:T(8,128)(2,1)} reshape(bf16[128,4,2048]{2,1,0:T(4,128)(2,1)S(1)} %all_to_all.26) | data formatting | bytes 4194304 | tf_op jit(solution)/shard_map/reshape | solution.py:80
  94.6 6.7 %fusion.4 = f32[512,1024]{1,0:T(8,128)} fusion(bf16[512,2048]{1,0:T(8,128)(2,1)} %reshape.191, bf16[1,2048,1024]{2,1,0:T(8,128)(2,1)} %param.23), kind=kOutput, calls=%fused_computation.6 | convolution fusion | flops 2147483648 | bytes 8388608 | tf_op jit(solution)/shard_map/dot_general | solution.py:81
  101.3 9.9 %fusion.6 = bf16[512,2048]{1,0:T(8,128)(2,1)} fusion(bf16[1,1024,2048]{2,1,0:T(8,128)(2,1)} %param.25, f32[512,1024]{1,0:T(8,128)} %fusion.4, bf16[512,2048]{1,0:T(8,128)(2,1)S(1)} %copy-done.1, bf16[1,2048,1024]{2,1,0:T(8,128)(2,1)} %param.24), kind=kOutput, calls=%fused_computation.8 | convolution fusion | flops 4299161600 | bytes 14680064 | tf_op jit(solution)/shard_map/dot_general | solution.py:84
  111.2 4.1 %reshape.192 = bf16[128,4,2048]{2,1,0:T(4,128)(2,1)} reshape(bf16[512,2048]{1,0:T(8,128)(2,1)} %fusion.6) | data formatting | bytes 4194304 | tf_op jit(solution)/shard_map/reshape | solution.py:88
  115.3 5.1 %all-to-all-start.2 = ((bf16[128,4,2048]{2,1,0:T(4,128)(2,1)}), bf16[128,4,2048]{2,1,0:T(4,128)(2,1)}, u32[]{:S(2)}, u32[]{:S(2)}) async-start(bf16[128,4,2048]{2,1,0:T(4,128)(2,1)} %reshape.192), calls=%async_computation.2 | async-start | bytes 4194304 | tf_op jit(solution)/shard_map/all_to_all | solution.py:87
  120.4 0.1 copy.22
  120.5 30.3 %all-to-all-done.2 = bf16[128,4,2048]{2,1,0:T(4,128)(2,1)} async-done(((bf16[128,4,2048]{2,1,0:T(4,128)(2,1)}), bf16[128,4,2048]{2,1,0:T(4,128)(2,1)}, u32[]{:S(2)}, u32[]{:S(2)}) %all-to-all-start.2) | async-done | bytes 2097184 | tf_op jit(solution)/shard_map/all_to_all | solution.py:87
  150.8 2.5 %reshape.193 = bf16[512,2048]{1,0:T(8,128)(2,1)S(1)} reshape(bf16[128,4,2048]{2,1,0:T(4,128)(2,1)} %all-to-all-done.2) | data formatting | bytes 4194304 | tf_op jit(solution)/shard_map/reshape | solution.py:90
  153.4 2.3 %gather_fusion = bf16[256,2048]{1,0:T(8,128)(2,1)} fusion(bf16[512,2048]{1,0:T(8,128)(2,1)S(1)} %reshape.193, s32[1024]{0:T(1024)S(1)} %pad_clamp_fusion), kind=kCustom, calls=%fused_computation | custom fusion | bytes 2098176 | tf_op jit(solution)/shard_map/gather | solution.py:90
  155.7 2.4 %reshape.203 = f32[128,2,2048]{2,1,0:T(2,128)S(1)} reshape(bf16[256,2048]{1,0:T(8,128)(2,1)} %gather_fusion) | data formatting | bytes 3145728 | tf_op jit(solution)/shard_map/convert_element_type | solution.py:93
  158.1 3.2 %multiply_reduce_fusion = f32[128,2048]{1,0:T(8,128)S(1)} fusion(f32[128,2,2048]{2,1,0:T(2,128)S(1)} %reshape.203, f32[128,2]{1,0:T(8,128)S(1)} %copy.22), kind=kLoop, calls=%fused_computation.10 | loop fusion | flops 786432 | bytes 3146752 | tf_op jit(solution)/shard_map/reduce_sum | solution.py:92
  161.3 0.4 fusion.25
  161.7 0.4 multiply_reduce_fusion.1
  162.1 1.3 multiply_convert_fusion.1
  (40 shorter events, 0.4 us)
Async XLA Ops:
  0.0 12.5 %copy-start = (f32[31,512]{1,0:T(8,128)S(1)}, f32[31,512]{1,0:T(8,128)}, u32[]{:S(2)}) copy-start(f32[31,512]{1,0:T(8,128)} %param.15) | copy-start | bytes 190468
  0.8 9.3 %collective-permute-start = (bf16[30,512]{1,0:T(8,128)(2,1)S(1)}, bf16[30,512]{1,0:T(8,128)(2,1)S(1)}, u32[]{:S(2)}, u32[]{:S(2)}) collective-permute-start(bf16[30,512]{1,0:T(8,128)(2,1)S(1)} %slice.12), channel_id=1, source_target_pairs={{0,4},{4,8},{8,12},{12,16},{16,20},{20,24},{24,28},{28,32},{32,36}... | collective-permute-start | bytes 92168 | tf_op jit(solution)/shard_map/ppermute | solution.py:12
  6.2 3.9 %collective-permute-start.1 = (bf16[30,512]{1,0:T(8,128)(2,1)S(1)}, bf16[30,512]{1,0:T(8,128)(2,1)S(1)}, u32[]{:S(2)}, u32[]{:S(2)}) collective-permute-start(bf16[30,512]{1,0:T(8,128)(2,1)S(1)} %slice.13), channel_id=1, source_target_pairs={{0,4},{4,8},{8,12},{12,16},{16,20},{20,24},{24,28},{28,32},{32,36}... | collective-permute-start | bytes 92168 | tf_op jit(solution)/shard_map/ppermute | solution.py:12
  11.7 0.8 copy-start.9
  16.5 9.2 %copy-start.8 = (f32[512]{0:T(512)S(1)}, f32[512]{0:T(512)}, u32[]{:S(2)}) copy-start(f32[512]{0:T(512)} %param.16) | copy-start | bytes 6148
  16.7 13.6 %copy-start.6 = (s32[128,2]{0,1:T(2,128)S(1)}, s32[128,2]{0,1:T(2,128)}, u32[]{:S(2)}) copy-start(s32[128,2]{0,1:T(2,128)} %param.21) | copy-start | bytes 3076
  16.7 13.8 %copy-start.3 = (s32[128,8,32]{0,1,2:T(8,128)S(1)}, s32[128,8,32]{0,1,2:T(8,128)}, u32[]{:S(2)}) copy-start(s32[128,8,32]{0,1,2:T(8,128)} %broadcast_add_fusion) | copy-start | bytes 393220
  17.1 20.2 %copy-start.2 = (bf16[128,2048]{1,0:T(8,128)(2,1)S(1)}, bf16[128,2048]{1,0:T(8,128)(2,1)}, u32[]{:S(2)}) copy-start(bf16[128,2048]{1,0:T(8,128)(2,1)} %param.18) | copy-start | bytes 1572868
  26.9 10.4 %all-to-all-start = ((bf16[4,128,512]{1,2,0:T(8,128)(2,1)}), bf16[4,128,512]{1,2,0:T(8,128)(2,1)S(1)}, u32[]{:S(2)}, u32[]{:S(2)}) async-start(bf16[4,128,512]{1,2,0:T(8,128)(2,1)} %multiply_convert_fusion.3), calls=%async_computation | async-start | bytes 1048576 | tf_op jit(solution)/shard_map/all_to_all | solution.py:58
  37.3 5.0 %copy-start.4 = (f32[2048]{0:T(1024)S(1)}, f32[2048]{0:T(1024)}, u32[]{:S(2)}) copy-start(f32[2048]{0:T(1024)} %param.19) | copy-start | bytes 24580
  94.6 6.7 %copy-start.1 = (bf16[512,2048]{1,0:T(8,128)(2,1)S(1)}, bf16[512,2048]{1,0:T(8,128)(2,1)}, u32[]{:S(2)}) copy-start(bf16[512,2048]{1,0:T(8,128)(2,1)} %reshape.191) | copy-start | bytes 6291460
  115.3 5.1 %copy-start.7 = (f32[128,2]{0,1:T(2,128)S(1)}, f32[128,2]{0,1:T(2,128)}, u32[]{:S(2)}) copy-start(f32[128,2]{0,1:T(2,128)} %param.22) | copy-start | bytes 3076
  115.3 35.5 %all-to-all-start.2 = ((bf16[128,4,2048]{2,1,0:T(4,128)(2,1)}), bf16[128,4,2048]{2,1,0:T(4,128)(2,1)}, u32[]{:S(2)}, u32[]{:S(2)}) async-start(bf16[128,4,2048]{2,1,0:T(4,128)(2,1)} %reshape.192), calls=%async_computation.2 | async-start | bytes 4194304 | tf_op jit(solution)/shard_map/all_to_all | solution.py:87
  161.3 0.8 copy-start.5
where the time goes:
time: 164 us; the launch traced here: 163 us
  blocking collectives  50.9 us (31%)
  waiting for transfers between devices  36.6 us (22%)
  local copies, waits for them, and re-layouts  26.9 us (16%)
  matrix products  23.7 us (14%)
  starting transfers between devices  15 us (9%)
  other arithmetic  9.94 us (6%)
    all_to_all x1, blocking collectives, per_device(): lax.all_to_all(outgoing, ('sp', 'tp'), split_axis=0, concat_axis=0, tiled...  42.3 us
    all_to_all x1, waiting for transfers between devices, per_device(): lax.all_to_all(answer.reshape(shape), ('sp', 'tp'), split_axis=0, concat_...  30.3 us
    dot_general x1, matrix products, per_device(): jnp.dot(hidden, expert_down[0], preferred_element_type=jnp.float32)  9.91 us
    psum x1, blocking collectives, per_device(): lax.psum((jnp.sum(conv, axis=1), jnp.sum(conv * conv, axis=1)), 'tp')  8.61 us
    dot_general x1, matrix products, per_device(): gate = jnp.dot(flat, expert_gate[0], preferred_element_type=jnp.float32)  6.65 us
    ppermute x2, starting transfers between devices, from_behind(): return lax.ppermute(block, axis, route)  6.5 us
    all_to_all x1, waiting for transfers between devices, per_device(): owned = lax.all_to_all(act, 'tp', split_axis=0, concat_axis=1, tiled=True)  6.27 us
    all_to_all x1, starting transfers between devices, per_device(): lax.all_to_all(answer.reshape(shape), ('sp', 'tp'), split_axis=0, concat_...  5.06 us
  transfers between devices with their start and end apart: 4, of which 2 were waited for; matrix products, arithmetic and copies ran while one was open for 2% of the time, Pallas kernels for 0%

commit v1 on v0

v1 whole, which is shorter than its diff:
```python
import functools

import jax
import jax.numpy as jnp
from jax import lax
from jax.experimental import pallas as pl
from jax.experimental.pallas import tpu as pltpu
from jax.sharding import PartitionSpec as P

residual_scale = 8.0**0.25
MESH = pl.DeviceIdType.MESH
f32, bf16 = jnp.float32, jnp.bfloat16

PEERS, SLOTS, QUARTERS = 128, 4, 4
BLOCK = SLOTS * QUARTERS
HALF = PEERS // 2


def from_behind(block, axis, distance):
    devices = range(lax.axis_size(axis))
    route = [(i - distance, i) for i in devices if i - distance in devices]
    return lax.ppermute(block, axis, route)


def token_norm(values, gain):
    middle = jnp.mean(values, axis=-1, keepdims=True)
    centred = values - middle
    spread = jnp.mean(centred * centred, axis=-1, keepdims=True)
    return centred * lax.rsqrt(spread + 1e-05) * gain


def place():
    sp, x = lax.axis_index("sp"), lax.axis_index("tp")
    return x, (sp // 2) % 4, sp // 8, sp % 2


def partner(n, sign):
    x, y, z, c = place()
    dx, dy, dz, dc = n % 4, (n // 4) % 4, (n // 16) % 4, n // 64
    px, py, pz, pc = (x + sign * dx + 4) % 4, (y + sign * dy + 4) % 4, (z + sign * dz + 4) % 4, (c + dc) % 2
    return {"sp": (pz * 4 + py) * 2 + pc, "tp": px}


def offset_of(e):
    x, y, z, c = place()
    ex, ec, ey, ez = e & 3, (e >> 2) & 1, (e >> 3) & 3, e >> 5
    return ((ec - c) & 1) * 64 + ((ez - z) & 3) * 16 + ((ey - y) & 3) * 4 + ((ex - x) & 3)


def slot_rows(mine, other, earlier, axis):
    return jnp.sum(((mine == other) & earlier).astype(f32), axis=axis, keepdims=True).astype(jnp.int32)


def moe_kernel(
    first_ref,
    routes_ref,
    routes_t_ref,
    score_ref,
    gain_ref,
    gate_hbm,
    up_hbm,
    down_hbm,
    out_ref,
    gate_w,
    up_w,
    down_w,
    send,
    recv,
    flat,
    hidden,
    answer,
    back_send,
    back_recv,
    pick,
    total,
    w_sem,
    send_sem,
    recv_sem,
    back_send_sem,
    back_recv_sem,
):
    barrier = pltpu.get_barrier_semaphore()

    def greet(k, carry):
        pl.semaphore_signal(barrier, inc=1, device_id=partner(k, 1), device_id_type=MESH)
        return carry

    lax.fori_loop(1, PEERS, greet, 0)
    weights = [
        pltpu.make_async_copy(gate_hbm.at[0], gate_w, w_sem.at[0]),
        pltpu.make_async_copy(up_hbm.at[0], up_w, w_sem.at[1]),
        pltpu.make_async_copy(down_hbm.at[0], down_w, w_sem.at[2]),
    ]
    for copy in weights:
        copy.start()

    rows, width = first_ref.shape
    quarter = width // QUARTERS
    col = [routes_ref[:, k : k + 1] for k in range(2)]
    row = [routes_t_ref[k : k + 1, :] for k in range(2)]
    r_id = lax.broadcasted_iota(jnp.int32, (rows, rows), 0)
    c_id = lax.broadcasted_iota(jnp.int32, (rows, rows), 1)
    every = r_id >= 0
    before_l = [
        slot_rows(row[0], col[0], r_id < c_id, 0),
        slot_rows(row[1], col[0], every, 0) + slot_rows(row[1], col[1], r_id < c_id, 0),
    ]
    before_s = [
        slot_rows(col[0], row[0], c_id < r_id, 1),
        slot_rows(col[1], row[0], every, 1) + slot_rows(col[1], row[1], c_id < r_id, 1),
    ]
    where_l = [offset_of(row[k]) * BLOCK + before_l[k] for k in range(2)]
    where_s = [offset_of(col[k]) * BLOCK + before_s[k] for k in range(2)]

    stacked = jnp.concatenate([first_ref[:, q * quarter : (q + 1) * quarter] for q in range(QUARTERS)], axis=0)
    key_l = [jnp.concatenate([where_l[k] + q * SLOTS for q in range(QUARTERS)], axis=1) for k in range(2)]

    def fill(b, carry):
        ids = lax.broadcasted_iota(jnp.int32, (512, QUARTERS * rows), 0) + b * 512
        chosen = ((ids == key_l[0]) | (ids == key_l[1])).astype(f32).astype(bf16)
        picked = jnp.dot(chosen, stacked, preferred_element_type=f32).astype(bf16)
        send[pl.ds(pl.multiple_of(b * 32, 32), 32)] = picked.reshape(32, BLOCK, quarter)
        return carry

    lax.fori_loop(0, PEERS * BLOCK // 512, fill, 0)
    recv[0] = send[0]
    pl.semaphore_wait(barrier, PEERS - 1)

    def dispatch_to(n, h):
        return pltpu.make_async_remote_copy(
            src_ref=send.at[n],
            dst_ref=recv.at[n],
            send_sem=send_sem,
            recv_sem=recv_sem.at[h],
            device_id=partner(n, 1),
            device_id_type=MESH,
        )

    def answer_to(n, h):
        return pltpu.make_async_remote_copy(
            src_ref=back_send.at[n],
            dst_ref=back_recv.at[n],
            send_sem=back_send_sem,
            recv_sem=back_recv_sem.at[h],
            device_id=partner(n, -1),
            device_id_type=MESH,
        )

    def near(k, carry):
        dispatch_to((k * 37) % HALF, 0).start()
        return carry

    def far(k, carry):
        dispatch_to(HALF + (k * 37) % HALF, 1).start()
        return carry

    lax.fori_loop(1, HALF, near, 0)
    lax.fori_loop(0, HALF, far, 0)

    i = lax.broadcasted_iota(jnp.int32, (256, 256), 0)
    j = lax.broadcasted_iota(jnp.int32, (256, 256), 1)
    to_flat = (((i // 4) % 16) * 16 + (i // 64) * 4 + i % 4 == j).astype(f32).astype(bf16)
    to_block = (((j // 4) % 16) * 16 + (j // 64) * 4 + j % 4 == i).astype(f32).astype(bf16)

    for h in range(2):
        start = h * HALF
        own = 1 - h
        landed = recv.at[pl.ds(start + own, HALF - own)]
        pltpu.make_async_copy(landed, landed, recv_sem.at[h]).wait()
        for g in range(4):
            block = recv[pl.ds(start + g * 16, 16)].reshape(256, quarter)
            moved = jnp.dot(to_flat, block, preferred_element_type=f32).astype(bf16)
            for q in range(QUARTERS):
                flat[pl.ds(g * 64, 64), pl.ds(q * quarter, quarter)] = moved[q * 64 : (q + 1) * 64]
        if h == 0:
            for copy in weights:
                copy.wait()

        def hide(b, carry):
            cols = pl.ds(pl.multiple_of(b * 256, 256), 256)
            gate = jnp.dot(flat[...], gate_w[:, cols], preferred_element_type=f32)
            upper = jnp.dot(flat[...], up_w[:, cols], preferred_element_type=f32)
            hidden[:, cols] = (gate * jax.nn.sigmoid(gate) * upper).astype(bf16)
            return carry

        lax.fori_loop(0, hidden.shape[1] // 256, hide, 0)
        for q in range(QUARTERS):
            cols = pl.ds(q * quarter, quarter)
            result = jnp.dot(hidden[...], down_w[:, cols], preferred_element_type=f32).astype(bf16)
            for g in range(4):
                answer[g, pl.ds(q * 64, 64), :] = result[g * 64 : (g + 1) * 64]
        for g in range(4):
            moved = jnp.dot(to_block, answer[g], preferred_element_type=f32).astype(bf16)
            back_send[pl.ds(start + g * 16, 16)] = moved.reshape(16, BLOCK, quarter)
        if h == 0:
            back_recv[0] = back_send[0]

            def near_back(k, carry):
                answer_to((k * 37) % HALF, 0).start()
                return carry

            lax.fori_loop(1, HALF, near_back, 0)
        else:

            def far_back(k, carry):
                answer_to(HALF + (k * 37) % HALF, 1).start()
                return carry

            lax.fori_loop(0, HALF, far_back, 0)

    def choose(b, carry):
        ids = lax.broadcasted_iota(jnp.int32, (rows, PEERS * BLOCK), 1)
        k, q = b // QUARTERS, b % QUARTERS
        key = jnp.where(k == 0, where_s[0], where_s[1]) + q * SLOTS
        pick[pl.ds(pl.multiple_of(b * rows, rows), rows)] = (ids == key).astype(f32).astype(bf16)
        return carry

    lax.fori_loop(0, 2 * QUARTERS, choose, 0)

    for h in range(2):
        start = h * HALF
        own = 1 - h
        landed = back_recv.at[pl.ds(start + own, HALF - own)]
        pltpu.make_async_copy(landed, landed, back_recv_sem.at[h]).wait()
        block = back_recv[pl.ds(start, HALF)].reshape(HALF * BLOCK, quarter)
        part = jnp.dot(
            pick[:, pl.ds(start * BLOCK, HALF * BLOCK)], block, preferred_element_type=f32
        )
        total[...] = part if h == 0 else total[...] + part

    score = score_ref[...]
    share = score / (score[:, 0:1] + score[:, 1:2])
    mixed = []
    for q in range(QUARTERS):
        base = residual_scale * first_ref[:, q * quarter : (q + 1) * quarter].astype(f32)
        one = total[pl.ds(q * rows, rows), :] * share[:, 0:1]
        two = total[pl.ds((QUARTERS + q) * rows, rows), :] * share[:, 1:2]
        mixed.append(base + (one + two))
    middle = sum(jnp.sum(m, axis=1, keepdims=True) for m in mixed) / width
    mixed = [m - middle for m in mixed]
    spread = sum(jnp.sum(m * m, axis=1, keepdims=True) for m in mixed) / width
    scale = lax.rsqrt(spread + 1e-05)
    for q in range(QUARTERS):
        cols = slice(q * quarter, (q + 1) * quarter)
        out_ref[:, cols] = (mixed[q] * scale * gain_ref[:, cols]).astype(bf16)

    sent = send.at[pl.ds(1, PEERS - 1)]
    pltpu.make_async_copy(sent, sent, send_sem).wait()
    sent = back_send.at[pl.ds(1, PEERS - 1)]
    pltpu.make_async_copy(sent, sent, back_send_sem).wait()


def experts_layer(first, routes, score, gain, expert_gate, expert_up, expert_down):
    rows, width = first.shape
    inner = expert_gate.shape[2]
    quarter = width // QUARTERS
    vmem = pl.BlockSpec(memory_space=pltpu.VMEM)
    hbm = pl.BlockSpec(memory_space=pl.ANY)
    blocks = pltpu.VMEM((PEERS, BLOCK, quarter), bf16)
    return pl.pallas_call(
        moe_kernel,
        out_shape=jax.ShapeDtypeStruct((rows, width), bf16),
        in_specs=[vmem] * 5 + [hbm] * 3,
        out_specs=vmem,
        scratch_shapes=[
            pltpu.VMEM((width, inner), bf16),
            pltpu.VMEM((width, inner), bf16),
            pltpu.VMEM((inner, width), bf16),
            blocks,
            blocks,
            pltpu.VMEM((HALF * SLOTS, width), bf16),
            pltpu.VMEM((HALF * SLOTS, inner), bf16),
            pltpu.VMEM((4, 256, quarter), bf16),
            blocks,
            blocks,
            pltpu.VMEM((2 * QUARTERS * rows, PEERS * BLOCK), bf16),
            pltpu.VMEM((2 * QUARTERS * rows, quarter), f32),
            pltpu.SemaphoreType.DMA((3,)),
            pltpu.SemaphoreType.DMA,
            pltpu.SemaphoreType.DMA((2,)),
            pltpu.SemaphoreType.DMA,
            pltpu.SemaphoreType.DMA((2,)),
        ],
        compiler_params=pltpu.CompilerParams(
            collective_id=1, has_side_effects=True, vmem_limit_bytes=56 * 1024 * 1024
        ),
        name="experts",
    )(first, routes, routes.T, score, gain.reshape(1, -1), expert_gate, expert_up, expert_down)


def per_device(
    conv_value,
    conv_gate,
    conv_taps,
    channel_gain,
    point_weight,
    residual_in,
    first_gain,
    second_gain,
    routes,
    route_score,
    expert_gate,
    expert_up,
    expert_down,
):
    edge = conv_taps.shape[0] - 1
    local_width = conv_value.shape[1]
    rim_value, rim_gate = from_behind((conv_value[-edge:], conv_gate[-edge:]), "sp", 1)
    ext_value = jnp.concatenate([rim_value, conv_value], axis=0)
    ext_gate = jnp.concatenate([rim_gate, conv_gate], axis=0)
    glu = ext_value.astype(jnp.float32) * jax.nn.sigmoid(ext_gate.astype(jnp.float32))
    conv = lax.conv_general_dilated(
        glu[None],
        conv_taps[:, None, :],
        (1,),
        [(0, 0)],
        dimension_numbers=("NWC", "WIO", "NWC"),
        feature_group_count=local_width,
    )[0]
    width = local_width * lax.axis_size("tp")
    sums, squares = lax.psum((jnp.sum(conv, axis=1), jnp.sum(conv * conv, axis=1)), "tp")
    middle = sums / width
    spread = squares / width - middle * middle
    normed = (conv - middle[:, None]) * lax.rsqrt(spread + 1e-05)[:, None] * channel_gain
    act = (normed * jax.nn.sigmoid(normed)).astype(jnp.bfloat16)
    owned = lax.all_to_all(act, "tp", split_axis=0, concat_axis=1, tiled=True)
    mix = jnp.dot(owned, point_weight, preferred_element_type=jnp.float32)
    first = token_norm(residual_scale * residual_in.astype(jnp.float32) + mix, first_gain).astype(
        jnp.bfloat16
    )
    return experts_layer(first, routes, route_score, second_gain, expert_gate, expert_up, expert_down)


def solution(mesh):
    in_specs = (
        P("sp", "tp"),
        P("sp", "tp"),
        P(None, "tp"),
        P("tp"),
        P(),
        P(("sp", "tp"), None),
        P(),
        P(),
        P(("sp", "tp"), None),
        P(("sp", "tp"), None),
        P(("sp", "tp"), None, None),
        P(("sp", "tp"), None, None),
        P(("sp", "tp"), None, None),
    )
    out_specs = P(("sp", "tp"), None)
    return jax.shard_map(
        per_device, mesh=mesh, in_specs=in_specs, out_specs=out_specs, check_vma=False
    )
```

time: 164 us -> 131 us (0.80)
  Pallas kernels: 0 us -> 67.9 us
  blocking collectives: 50.9 us -> 8.47 us
  waiting for transfers between devices: 36.6 us -> 6.57 us
  local copies, waits for them, and re-layouts: 26.9 us -> 5.34 us
  other arithmetic: 9.94 us -> 4.08 us
  starting transfers between devices: 15 us -> 10.2 us
  matrix products: 23.7 us -> 28.1 us
    pallas_call x0 -> x1, Pallas kernels: none -> 67.9 us  [experts_layer(): pl.pallas_call(moe_kernel, out_shape=jax.ShapeDtypeStruct((rows, width),...]
    all_to_all x1 -> x0, blocking collectives: 42.3 us -> none  [per_device(): lax.all_to_all(outgoing, ('sp', 'tp'), split_axis=0, concat_axis=0, tiled...]
    all_to_all x1 -> x0, waiting for transfers between devices: 30.3 us -> none  [per_device(): lax.all_to_all(answer.reshape(shape), ('sp', 'tp'), split_axis=0, concat_...]
    conv_general_dilated x1, matrix products: 2.42 us -> 23.4 us  [per_device(): lax.conv_general_dilated(glu[None], conv_taps[:, None, :], (1,), [(0, 0)]...]
    dot_general x2 -> x0, matrix products: 16.6 us -> none  [the longest x1 9.91 us: per_device(): jnp.dot(hidden, expert_down[0], preferred_element_type=jnp.float32)]
    reshape x5 -> x0, local copies, waits for them, and re-layouts: 12.1 us -> none  [the longest x1 4.11 us: per_device(): answer.reshape(shape)]
    all_to_all x1 -> x0, starting transfers between devices: 5.06 us -> none  [per_device(): lax.all_to_all(answer.reshape(shape), ('sp', 'tp'), split_axis=0, concat_...]
    reduce_sum x5 -> x0, other arithmetic: 3.98 us -> none  [the longest x1 3.16 us: per_device(): jnp.sum(share[:, :, None] * per_assign.reshape(rows, top, model_width).as...]
  transfers between devices with their start and end apart: 4 -> 3, of which waited for: 2 -> 2; matrix products, arithmetic and copies ran while one was open for 2% -> 2% of each run, Pallas kernels for 0% -> 0%
where the time goes in v1:
time: 131 us
  Pallas kernels  67.9 us (52%)
  matrix products  28.1 us (21%)
  starting transfers between devices  10.2 us (8%)
  blocking collectives  8.47 us (6%)
  waiting for transfers between devices  6.57 us (5%)
  local copies, waits for them, and re-layouts  5.34 us (4%)
  other arithmetic  4.08 us (3%)
    pallas_call x1, Pallas kernels, experts_layer(): pl.pallas_call(moe_kernel, out_shape=jax.ShapeDtypeStruct((rows, width),...  67.9 us
    conv_general_dilated x1, matrix products, per_device(): lax.conv_general_dilated(glu[None], conv_taps[:, None, :], (1,), [(0, 0)]...  23.4 us
    psum x1, blocking collectives, per_device(): lax.psum((jnp.sum(conv, axis=1), jnp.sum(conv * conv, axis=1)), 'tp')  8.47 us
    ppermute x2, starting transfers between devices, from_behind(): return lax.ppermute(block, axis, route)  6.5 us
    all_to_all x1, waiting for transfers between devices, per_device(): owned = lax.all_to_all(act, 'tp', split_axis=0, concat_axis=1, tiled=True)  5.41 us
    dot_general x1, matrix products, per_device(): mix = jnp.dot(owned, point_weight, preferred_element_type=jnp.float32)  4.75 us
    all_to_all x1, starting transfers between devices, per_device(): owned = lax.all_to_all(act, 'tp', split_axis=0, concat_axis=1, tiled=True)  3.65 us
    unnamed x16, local copies, waits for them, and re-layouts  3.44 us
  transfers between devices with their start and end apart: 3, of which 2 were waited for; matrix products, arithmetic and copies ran while one was open for 2% of the time, Pallas kernels for 0%

profile of v1, /device:TPU:1, one launch (start us, length us, event | category | flops | bytes accessed | tf_op | source)
XLA Modules:
  0.0 130.8 jit_solution(3431950495355748344)
XLA Ops:
  0.0 0.0 copy-start
  0.0 0.8 slice.6
  0.8 4.6 %collective-permute-start = (bf16[30,512]{1,0:T(8,128)(2,1)S(1)}, bf16[30,512]{1,0:T(8,128)(2,1)S(1)}, u32[]{:S(2)}, u32[]{:S(2)}) collective-permute-start(bf16[30,512]{1,0:T(8,128)(2,1)S(1)} %slice.6), channel_id=1, source_target_pairs={{0,4},{4,8},{8,12},{12,16},{16,20},{20,24},{24,28},{28,32},{32,36}... | collective-permute-start | bytes 92168 | tf_op jit(solution)/shard_map/ppermute | solution.py:22
  5.4 0.8 slice.7
  6.2 1.9 %collective-permute-start.1 = (bf16[30,512]{1,0:T(8,128)(2,1)S(1)}, bf16[30,512]{1,0:T(8,128)(2,1)S(1)}, u32[]{:S(2)}, u32[]{:S(2)}) collective-permute-start(bf16[30,512]{1,0:T(8,128)(2,1)S(1)} %slice.7), channel_id=1, source_target_pairs={{0,4},{4,8},{8,12},{12,16},{16,20},{20,24},{24,28},{28,32},{32,36}... | collective-permute-start | bytes 92168 | tf_op jit(solution)/shard_map/ppermute | solution.py:22
  8.1 0.0 collective-permute-done
  8.1 1.2 collective-permute-done.1
  9.3 1.6 %divide_multiply_fusion = bf16[1,542,512]{2,1,0:T(8,128)(2,1)S(1)} fusion(bf16[1,512,512]{2,1,0:T(8,128)(2,1)} %bitcast.20, bf16[1,30,512]{2,1,0:T(8,128)(2,1)S(1)} %bitcast.22, bf16[1,512,512]{2,1,0:T(8,128)(2,1)} %bitcast.21, bf16[1,30,512]{2,1,0:T(8,128)(2,1)S(1)} %bitcast.23), kind=kLoop, calls=%fused_computation.1 | loop fusion | flops 3607552 | bytes 1665024 | tf_op jit(solution)/shard_map/mul | solution.py:311
  10.9 0.0 copy-done
  10.9 23.4 %fusion.3 = (f32[512]{0:T(512)S(1)}, f32[512]{0:T(512)S(1)}, f32[1,512,512]{2,0,1:T(1,128)S(1)}) fusion(f32[31,1,512]{2,0,1:T(8,128)S(1)} %bitcast.17, bf16[1,542,512]{2,1,0:T(8,128)(2,1)S(1)} %divide_multiply_fusion), kind=kOutput, calls=%fused_computation.13 | convolution fusion | flops 17038336 | bytes 1671168 | tf_op jit(solution)/shard_map/conv_general_dilated | solution.py:312
  34.3 0.1 copy.23
  34.4 0.0 copy-start.4
  34.4 0.3 copy.20
  34.7 8.5 %all-reduce = (f32[512]{0:T(512)S(1)}, f32[512]{0:T(512)S(1)}) all-reduce(f32[512]{0:T(512)S(1)} %get-tuple-element.6, f32[512]{0:T(512)S(1)} %get-tuple-element.5), channel_id=1, replica_groups=mesh['sp'=32,'tp'=4] {'tp'}, use_global_device_ids=true, to_apply=%region_3.0 | all-reduce | flops 1024 | bytes 8192 | tf_op jit(solution)/shard_map/psum | solution.py:321
  43.2 0.0 copy-done.4
  43.2 0.0 copy-start.3
  43.2 0.0 copy-start.5
  43.2 0.0 copy-start.1
  43.2 1.2 multiply_convert_fusion.1
  44.4 3.7 %all-to-all-start = ((bf16[4,128,512]{1,2,0:T(8,128)(2,1)}), bf16[4,128,512]{1,2,0:T(8,128)(2,1)S(1)}, u32[]{:S(2)}, u32[]{:S(2)}) async-start(bf16[4,128,512]{1,2,0:T(8,128)(2,1)} %multiply_convert_fusion.1), calls=%async_computation | async-start | bytes 1048576 | tf_op jit(solution)/shard_map/all_to_all | solution.py:326
  48.1 0.0 copy-done.3
  48.1 0.7 copy.21.routes_ref
  48.8 0.0 copy-done.5
  48.8 0.7 copy.22.score_ref
  49.5 5.4 %all-to-all-done = bf16[4,128,512]{1,2,0:T(8,128)(2,1)S(1)} async-done(((bf16[4,128,512]{1,2,0:T(8,128)(2,1)}), bf16[4,128,512]{1,2,0:T(8,128)(2,1)S(1)}, u32[]{:S(2)}, u32[]{:S(2)}) %all-to-all-start) | async-done | bytes 524320 | tf_op jit(solution)/shard_map/all_to_all | solution.py:326
  55.0 0.0 copy-done.1
  55.0 0.0 copy-start.2
  55.0 4.8 %fusion.4 = (f32[128]{0:T(128)S(1)}, f32[128,2048]{1,0:T(8,128)S(1)}) fusion(bf16[128,2048]{0,1:T(8,128)(2,1)S(1)} %bitcast.19, bf16[2048,2048]{1,0:T(8,128)(2,1)} %param.17, bf16[128,2048]{1,0:T(8,128)(2,1)S(1)} %copy-done.1), kind=kOutput, calls=%fused_computation.14 | convolution fusion | flops 1074790272 | bytes 10486272 | tf_op jit(solution)/shard_map/dot_general | solution.py:327
  59.7 0.3 multiply_reduce_fusion
  60.0 0.0 copy-done.2
  60.0 1.0 multiply_convert_fusion.first_ref
  61.0 67.9 %experts.1 = bf16[128,2048]{1,0:T(8,128)(2,1)} custom-call(bf16[128,2048]{1,0:T(8,128)(2,1)} %multiply_convert_fusion.first_ref, s32[128,2]{1,0:T(8,128)} %copy.21.routes_ref, s32[2,128]{1,0:T(2,128)} %bitcast.25, f32[128,2]{1,0:T(8,128)} %copy.22.score_ref, f32[1,2048]{1,0:T(1,128)} %bitcast.24, bf16[1,2048,1024]{2,1,0:T(8,128)(2,1)} %gate_hbm.1, ...), custom_call_target="tpu_custom_call" | custom-call | tf_op jit(solution)/shard_map/experts/pallas_call | solution.py:260
  129.0 1.9 %copy.33 = bf16[128,2048]{1,0:T(8,128)(2,1)} copy(bf16[128,2048]{1,0:T(8,128)(2,1)} %experts.1) | data formatting | bytes 1048576
  (3 shorter events, 0.0 us)
Async XLA Ops:
  0.0 10.9 %copy-start = (f32[31,512]{1,0:T(8,128)S(1)}, f32[31,512]{1,0:T(8,128)}, u32[]{:S(2)}) copy-start(f32[31,512]{1,0:T(8,128)} %param.15) | copy-start | bytes 190468
  0.8 7.3 %collective-permute-start = (bf16[30,512]{1,0:T(8,128)(2,1)S(1)}, bf16[30,512]{1,0:T(8,128)(2,1)S(1)}, u32[]{:S(2)}, u32[]{:S(2)}) collective-permute-start(bf16[30,512]{1,0:T(8,128)(2,1)S(1)} %slice.6), channel_id=1, source_target_pairs={{0,4},{4,8},{8,12},{12,16},{16,20},{20,24},{24,28},{28,32},{32,36}... | collective-permute-start | bytes 92168 | tf_op jit(solution)/shard_map/ppermute | solution.py:22
  6.2 3.1 %collective-permute-start.1 = (bf16[30,512]{1,0:T(8,128)(2,1)S(1)}, bf16[30,512]{1,0:T(8,128)(2,1)S(1)}, u32[]{:S(2)}, u32[]{:S(2)}) collective-permute-start(bf16[30,512]{1,0:T(8,128)(2,1)S(1)} %slice.7), channel_id=1, source_target_pairs={{0,4},{4,8},{8,12},{12,16},{16,20},{20,24},{24,28},{28,32},{32,36}... | collective-permute-start | bytes 92168 | tf_op jit(solution)/shard_map/ppermute | solution.py:22
  34.4 8.8 %copy-start.4 = (f32[512]{0:T(512)S(1)}, f32[512]{0:T(512)}, u32[]{:S(2)}) copy-start(f32[512]{0:T(512)} %param.16) | copy-start | bytes 6148
  43.2 4.9 %copy-start.3 = (s32[128,2]{0,1:T(2,128)S(1)}, s32[128,2]{0,1:T(2,128)}, u32[]{:S(2)}) copy-start(s32[128,2]{0,1:T(2,128)} %param.21) | copy-start | bytes 3076
  43.2 5.6 %copy-start.5 = (f32[128,2]{0,1:T(2,128)S(1)}, f32[128,2]{0,1:T(2,128)}, u32[]{:S(2)}) copy-start(f32[128,2]{0,1:T(2,128)} %param.22) | copy-start | bytes 3076
  43.2 11.7 %copy-start.1 = (bf16[128,2048]{1,0:T(8,128)(2,1)S(1)}, bf16[128,2048]{1,0:T(8,128)(2,1)}, u32[]{:S(2)}) copy-start(bf16[128,2048]{1,0:T(8,128)(2,1)} %param.18) | copy-start | bytes 1572868
  44.4 10.5 %all-to-all-start = ((bf16[4,128,512]{1,2,0:T(8,128)(2,1)}), bf16[4,128,512]{1,2,0:T(8,128)(2,1)S(1)}, u32[]{:S(2)}, u32[]{:S(2)}) async-start(bf16[4,128,512]{1,2,0:T(8,128)(2,1)} %multiply_convert_fusion.1), calls=%async_computation | async-start | bytes 1048576 | tf_op jit(solution)/shard_map/all_to_all | solution.py:326
  55.0 5.0 %copy-start.2 = (f32[2048]{0:T(1024)S(1)}, f32[2048]{0:T(1024)}, u32[]{:S(2)}) copy-start(f32[2048]{0:T(1024)} %param.19) | copy-start | bytes 24580

commit v2 on v1

v2 whole, which is shorter than its diff:
```python
import functools

import jax
import jax.numpy as jnp
from jax import lax
from jax.experimental import pallas as pl
from jax.experimental.pallas import tpu as pltpu
from jax.sharding import PartitionSpec as P

residual_scale = 8.0**0.25
MESH = pl.DeviceIdType.MESH
f32, bf16 = jnp.float32, jnp.bfloat16

PEERS, SLOTS, QUARTERS = 128, 4, 4
BLOCK = SLOTS * QUARTERS
HALF = PEERS // 2


def place():
    sp, x = lax.axis_index("sp"), lax.axis_index("tp")
    return x, (sp // 2) % 4, sp // 8, sp % 2


def partner(n, sign):
    x, y, z, c = place()
    dx, dy, dz, dc = n % 4, (n // 4) % 4, (n // 16) % 4, n // 64
    px, py, pz, pc = (x + sign * dx + 4) % 4, (y + sign * dy + 4) % 4, (z + sign * dz + 4) % 4, (c + dc) % 2
    return {"sp": (pz * 4 + py) * 2 + pc, "tp": px}


def offset_of(e):
    x, y, z, c = place()
    ex, ec, ey, ez = e & 3, (e >> 2) & 1, (e >> 3) & 3, e >> 5
    return ((ec - c) & 1) * 64 + ((ez - z) & 3) * 16 + ((ey - y) & 3) * 4 + ((ex - x) & 3)


def slot_rows(mine, other, earlier, axis):
    return jnp.sum(((mine == other) & earlier).astype(f32), axis=axis, keepdims=True).astype(jnp.int32)


def silu(values):
    return values * (1.0 / (1.0 + jnp.exp(-values)))


def across(row):
    n = row.shape[1]
    same = lax.broadcasted_iota(jnp.int32, (n, n), 0) == lax.broadcasted_iota(jnp.int32, (n, n), 1)
    return jnp.sum(jnp.where(same, row, jnp.zeros_like(row)), axis=1, keepdims=True)


def order_of_blocks():
    x = lax.axis_index("tp")
    table = ((2, 1, 3, 0), (3, 2, 0, 1), (3, 1, 0, 2), (1, 2, 0, 3))
    return [
        jnp.where(x == 0, table[0][k], jnp.where(x == 1, table[1][k], jnp.where(x == 2, table[2][k], table[3][k])))
        for k in range(4)
    ]


def layer_kernel(
    value_hbm,
    gate_in_hbm,
    taps_ref,
    channel_gain_ref,
    point_hbm,
    residual_hbm,
    first_gain_ref,
    routes_ref,
    score_ref,
    gate_hbm,
    up_hbm,
    down_hbm,
    out_ref,
    value,
    gate_in,
    rim,
    glu,
    conv_send,
    conv_own,
    conv_recv,
    gains,
    point,
    residual,
    act,
    h1,
    stacked,
    gate_w,
    up_w,
    down_w,
    send,
    recv,
    flat,
    hidden,
    answer,
    back_send,
    back_recv,
    pick,
    total,
    in_sem,
    w_sem,
    rim_sem,
    gain_sem,
    conv_sem,
    send_sem,
    recv_sem,
    back_send_sem,
    back_recv_sem,
):
    inputs = [
        pltpu.make_async_copy(value_hbm, value, in_sem.at[0]),
        pltpu.make_async_copy(gate_in_hbm, gate_in, in_sem.at[1]),
    ]
    weights = [
        pltpu.make_async_copy(point_hbm, point, w_sem.at[0]),
        pltpu.make_async_copy(residual_hbm, residual, w_sem.at[1]),
        pltpu.make_async_copy(gate_hbm.at[0], gate_w, w_sem.at[2]),
        pltpu.make_async_copy(up_hbm.at[0], up_w, w_sem.at[3]),
        pltpu.make_async_copy(down_hbm.at[0], down_w, w_sem.at[4]),
    ]
    for copy in inputs + weights:
        copy.start()
    barrier = pltpu.get_barrier_semaphore()

    def greet(k, carry):
        pl.semaphore_signal(barrier, inc=1, device_id=partner(k, 1), device_id_type=MESH)
        return carry

    lax.fori_loop(1, PEERS, greet, 0)

    rows, quarter = conv_own.shape
    width = quarter * QUARTERS
    taps_n = taps_ref.shape[0]
    lanes = glu.shape[3]
    chunks = quarter // lanes
    lead = glu.shape[2] - rows
    sp, x = lax.axis_index("sp"), lax.axis_index("tp")

    def put_glu(block, values, start):
        for cc in range(chunks):
            glu[block, cc, start : start + values.shape[0], :] = values[:, cc * lanes : (cc + 1) * lanes]

    for copy in inputs:
        copy.wait()
    for p in range(4):
        own = slice(p * rows, (p + 1) * rows)
        gated = value[own, :].astype(f32) * (1.0 / (1.0 + jnp.exp(-gate_in[own, :].astype(f32))))
        put_glu(p, gated, lead)
        if p < 3:
            put_glu(p + 1, gated[rows - lead :], 0)

    def convolve(p, into):
        for cc in range(chunks):
            cols = slice(cc * lanes, (cc + 1) * lanes)
            sum_ = jnp.zeros((rows, lanes), f32)
            for j in range(taps_n):
                sum_ = sum_ + taps_ref[j : j + 1, cols] * glu[p, cc, pl.ds(lead - taps_n + 1 + j, rows), :]
            into[:, cols] = sum_.astype(bf16)

    order = order_of_blocks()
    convolve(order[0], conv_send.at[0])
    pl.semaphore_wait(barrier, PEERS - 1)

    total_rows = value.shape[0]
    behind = {"sp": (sp + 1) % 32, "tp": x}
    rims = [
        pltpu.make_async_remote_copy(
            src_ref=ref.at[pl.ds(total_rows - lead, lead)],
            dst_ref=rim.at[i],
            send_sem=rim_sem.at[0],
            recv_sem=rim_sem.at[1],
            device_id=behind,
            device_id_type=MESH,
        )
        for i, ref in enumerate((value, gate_in))
    ]
    for copy in rims:
        copy.start()

    def conv_to(k):
        return pltpu.make_async_remote_copy(
            src_ref=conv_send.at[k],
            dst_ref=conv_recv.at[(x - order[k] + 4) % 4 - 1],
            send_sem=conv_sem.at[0],
            recv_sem=conv_sem.at[1],
            device_id={"sp": sp, "tp": order[k]},
            device_id_type=MESH,
        )

    def gain_to(d):
        return pltpu.make_async_remote_copy(
            src_ref=channel_gain_ref,
            dst_ref=gains.at[3 - d],
            send_sem=gain_sem.at[0],
            recv_sem=gain_sem.at[1],
            device_id={"sp": sp, "tp": (x + d) % 4},
            device_id_type=MESH,
        )

    conv_to(0).start()
    for d in range(1, 4):
        gain_to(d).start()
    convolve(order[1], conv_send.at[1])
    conv_to(1).start()
    pltpu.make_async_copy(rim, rim, rim_sem.at[1]).wait()
    gated = rim[0].astype(f32) * (1.0 / (1.0 + jnp.exp(-rim[1].astype(f32))))
    put_glu(0, jnp.where(sp > 0, gated, jnp.zeros_like(gated)), 0)
    convolve(order[2], conv_send.at[2])
    conv_to(2).start()
    convolve(order[3], conv_own)

    row = [routes_ref[k : k + 1, :] for k in range(2)]
    col = [across(r) for r in row]
    r_id = lax.broadcasted_iota(jnp.int32, (rows, rows), 0)
    c_id = lax.broadcasted_iota(jnp.int32, (rows, rows), 1)
    every = r_id >= 0
    before_l = [
        slot_rows(row[0], col[0], r_id < c_id, 0),
        slot_rows(row[1], col[0], every, 0) + slot_rows(row[1], col[1], r_id < c_id, 0),
    ]
    before_s = [
        slot_rows(col[0], row[0], c_id < r_id, 1),
        slot_rows(col[1], row[0], every, 1) + slot_rows(col[1], row[1], c_id < r_id, 1),
    ]
    where_l = [offset_of(row[k]) * BLOCK + before_l[k] for k in range(2)]
    where_s = [offset_of(col[k]) * BLOCK + before_s[k] for k in range(2)]
    key_l = [jnp.concatenate([where_l[k] + q * SLOTS for q in range(QUARTERS)], axis=1) for k in range(2)]

    def choose(b, carry):
        ids = lax.broadcasted_iota(jnp.int32, (rows, PEERS * BLOCK), 1)
        k, q = b // QUARTERS, b % QUARTERS
        key = jnp.where(k == 0, where_s[0], where_s[1]) + q * SLOTS
        pick[pl.ds(pl.multiple_of(b * rows, rows), rows)] = (ids == key).astype(f32).astype(bf16)
        return carry

    lax.fori_loop(0, 2 * QUARTERS, choose, 0)

    pltpu.make_async_copy(conv_recv, conv_recv, conv_sem.at[1]).wait()
    pltpu.make_async_copy(gains, gains, gain_sem.at[1]).wait()
    parts = [conv_own[...].astype(f32)] + [conv_recv[i].astype(f32) for i in range(3)]
    middle = sum(jnp.sum(v, axis=1, keepdims=True) for v in parts) / width
    spread = sum(jnp.sum(v * v, axis=1, keepdims=True) for v in parts) / width - middle * middle
    scale = lax.rsqrt(spread + 1e-05)
    for i in range(4):
        gain = channel_gain_ref[...] if i == 0 else gains[i - 1]
        act[i] = silu((parts[i] - middle) * scale * gain).astype(bf16)
    for copy in weights[:2]:
        copy.wait()

    def mix(b, carry):
        cols = pl.ds(pl.multiple_of(b * quarter, quarter), quarter)
        sum_ = residual_scale * residual[:, cols].astype(f32)
        for i in range(4):
            block = (x + i) % 4
            sum_ = sum_ + jnp.dot(
                act[i],
                point[pl.ds(pl.multiple_of(block * quarter, quarter), quarter), cols],
                preferred_element_type=f32,
            )
        h1[b] = sum_
        return carry

    lax.fori_loop(0, QUARTERS, mix, 0)
    middle = sum(jnp.sum(h1[q], axis=1, keepdims=True) for q in range(QUARTERS)) / width
    centred = [h1[q] - middle for q in range(QUARTERS)]
    spread = sum(jnp.sum(v * v, axis=1, keepdims=True) for v in centred) / width
    scale = lax.rsqrt(spread + 1e-05)
    for q in range(QUARTERS):
        cols = slice(q * quarter, (q + 1) * quarter)
        stacked[pl.ds(q * rows, rows), :] = (centred[q] * scale * first_gain_ref[:, cols]).astype(bf16)

    def fill(b, carry):
        ids = lax.broadcasted_iota(jnp.int32, (512, QUARTERS * rows), 0) + b * 512
        chosen = ((ids == key_l[0]) | (ids == key_l[1])).astype(f32).astype(bf16)
        picked = jnp.dot(chosen, stacked[...], preferred_element_type=f32).astype(bf16)
        send[pl.ds(pl.multiple_of(b * 32, 32), 32)] = picked.reshape(32, BLOCK, quarter)
        return carry

    lax.fori_loop(0, PEERS * BLOCK // 512, fill, 0)
    recv[0] = send[0]
    def dispatch_to(n, h):
        return pltpu.make_async_remote_copy(
            src_ref=send.at[n],
            dst_ref=recv.at[n],
            send_sem=send_sem,
            recv_sem=recv_sem.at[h],
            device_id=partner(n, 1),
            device_id_type=MESH,
        )

    def answer_to(n, h):
        return pltpu.make_async_remote_copy(
            src_ref=back_send.at[n],
            dst_ref=back_recv.at[n],
            send_sem=back_send_sem,
            recv_sem=back_recv_sem.at[h],
            device_id=partner(n, -1),
            device_id_type=MESH,
        )

    def near(k, carry):
        dispatch_to((k * 37) % HALF, 0).start()
        return carry

    def far(k, carry):
        dispatch_to(HALF + (k * 37) % HALF, 1).start()
        return carry

    lax.fori_loop(1, HALF, near, 0)
    lax.fori_loop(0, HALF, far, 0)

    i = lax.broadcasted_iota(jnp.int32, (256, 256), 0)
    j = lax.broadcasted_iota(jnp.int32, (256, 256), 1)
    to_flat = (((i // 4) % 16) * 16 + (i // 64) * 4 + i % 4 == j).astype(f32).astype(bf16)
    to_block = (((j // 4) % 16) * 16 + (j // 64) * 4 + j % 4 == i).astype(f32).astype(bf16)

    for h in range(2):
        start = h * HALF
        own = 1 - h
        landed = recv.at[pl.ds(start + own, HALF - own)]
        pltpu.make_async_copy(landed, landed, recv_sem.at[h]).wait()
        for g in range(4):
            block = recv[pl.ds(start + g * 16, 16)].reshape(256, quarter)
            moved = jnp.dot(to_flat, block, preferred_element_type=f32).astype(bf16)
            for q in range(QUARTERS):
                flat[pl.ds(g * 64, 64), pl.ds(q * quarter, quarter)] = moved[q * 64 : (q + 1) * 64]
        if h == 0:
            for copy in weights[2:]:
                copy.wait()

        def hide(b, carry):
            cols = pl.ds(pl.multiple_of(b * 256, 256), 256)
            gate = jnp.dot(flat[...], gate_w[:, cols], preferred_element_type=f32)
            upper = jnp.dot(flat[...], up_w[:, cols], preferred_element_type=f32)
            hidden[:, cols] = (gate * jax.nn.sigmoid(gate) * upper).astype(bf16)
            return carry

        lax.fori_loop(0, hidden.shape[1] // 256, hide, 0)
        for q in range(QUARTERS):
            cols = pl.ds(q * quarter, quarter)
            result = jnp.dot(hidden[...], down_w[:, cols], preferred_element_type=f32).astype(bf16)
            for g in range(4):
                answer[g, pl.ds(q * 64, 64), :] = result[g * 64 : (g + 1) * 64]
        for g in range(4):
            moved = jnp.dot(to_block, answer[g], preferred_element_type=f32).astype(bf16)
            back_send[pl.ds(start + g * 16, 16)] = moved.reshape(16, BLOCK, quarter)
        if h == 0:
            back_recv[0] = back_send[0]

            def near_back(k, carry):
                answer_to((k * 37) % HALF, 0).start()
                return carry

            lax.fori_loop(1, HALF, near_back, 0)
        else:

            def far_back(k, carry):
                answer_to(HALF + (k * 37) % HALF, 1).start()
                return carry

            lax.fori_loop(0, HALF, far_back, 0)

    for h in range(2):
        start = h * HALF
        own = 1 - h
        landed = back_recv.at[pl.ds(start + own, HALF - own)]
        pltpu.make_async_copy(landed, landed, back_recv_sem.at[h]).wait()
        block = back_recv[pl.ds(start, HALF)].reshape(HALF * BLOCK, quarter)
        part = jnp.dot(
            pick[:, pl.ds(start * BLOCK, HALF * BLOCK)], block, preferred_element_type=f32
        )
        total[...] = part if h == 0 else total[...] + part

    share = [across(score_ref[k : k + 1, :] / (score_ref[0:1, :] + score_ref[1:2, :])) for k in range(2)]
    mixed = []
    for q in range(QUARTERS):
        base = residual_scale * stacked[pl.ds(q * rows, rows), :].astype(f32)
        one = total[pl.ds(q * rows, rows), :] * share[0]
        two = total[pl.ds((QUARTERS + q) * rows, rows), :] * share[1]
        mixed.append(base + (one + two))
    middle = sum(jnp.sum(m, axis=1, keepdims=True) for m in mixed) / width
    mixed = [m - middle for m in mixed]
    spread = sum(jnp.sum(m * m, axis=1, keepdims=True) for m in mixed) / width
    scale = lax.rsqrt(spread + 1e-05)
    for q in range(QUARTERS):
        out_ref[:, q * quarter : (q + 1) * quarter] = mixed[q] * scale

    for copy in rims:
        copy.wait_send()
    for k in range(3):
        conv_to(k).wait_send()
    for d in range(1, 4):
        gain_to(d).wait_send()
    sent = send.at[pl.ds(1, PEERS - 1)]
    pltpu.make_async_copy(sent, sent, send_sem).wait()
    sent = back_send.at[pl.ds(1, PEERS - 1)]
    pltpu.make_async_copy(sent, sent, back_send_sem).wait()


def per_device(
    conv_value,
    conv_gate,
    conv_taps,
    channel_gain,
    point_weight,
    residual_in,
    first_gain,
    second_gain,
    routes,
    route_score,
    expert_gate,
    expert_up,
    expert_down,
):
    rows, width = residual_in.shape
    inner = expert_gate.shape[2]
    tokens, quarter = conv_value.shape
    lanes = 128
    lead = -(-(conv_taps.shape[0] - 1) // 16) * 16
    vmem = pl.BlockSpec(memory_space=pltpu.VMEM)
    hbm = pl.BlockSpec(memory_space=pl.ANY)
    blocks = pltpu.VMEM((PEERS, BLOCK, quarter), bf16)
    dma = pltpu.SemaphoreType.DMA
    normed = pl.pallas_call(
        layer_kernel,
        out_shape=jax.ShapeDtypeStruct((rows, width), f32),
        in_specs=[hbm, hbm, vmem, vmem, hbm, hbm, vmem, vmem, vmem, hbm, hbm, hbm],
        out_specs=vmem,
        scratch_shapes=[
            pltpu.VMEM((tokens, quarter), bf16),
            pltpu.VMEM((tokens, quarter), bf16),
            pltpu.VMEM((2, lead, quarter), bf16),
            pltpu.VMEM((4, quarter // lanes, lead + rows, lanes), f32),
            pltpu.VMEM((3, rows, quarter), bf16),
            pltpu.VMEM((rows, quarter), bf16),
            pltpu.VMEM((3, rows, quarter), bf16),
            pltpu.VMEM((3, 1, quarter), f32),
            pltpu.VMEM((width, width), bf16),
            pltpu.VMEM((rows, width), bf16),
            pltpu.VMEM((4, rows, quarter), bf16),
            pltpu.VMEM((QUARTERS, rows, quarter), f32),
            pltpu.VMEM((QUARTERS * rows, quarter), bf16),
            pltpu.VMEM((width, inner), bf16),
            pltpu.VMEM((width, inner), bf16),
            pltpu.VMEM((inner, width), bf16),
            blocks,
            blocks,
            pltpu.VMEM((HALF * SLOTS, width), bf16),
            pltpu.VMEM((HALF * SLOTS, inner), bf16),
            pltpu.VMEM((4, 256, quarter), bf16),
            blocks,
            blocks,
            pltpu.VMEM((2 * QUARTERS * rows, PEERS * BLOCK), bf16),
            pltpu.VMEM((2 * QUARTERS * rows, quarter), f32),
            dma((2,)),
            dma((5,)),
            dma((2,)),
            dma((2,)),
            dma((2,)),
            dma,
            dma((2,)),
            dma,
            dma((2,)),
        ],
        compiler_params=pltpu.CompilerParams(
            collective_id=1, has_side_effects=True, vmem_limit_bytes=60 * 1024 * 1024
        ),
        name="layer",
    )(
        conv_value,
        conv_gate,
        conv_taps,
        channel_gain.reshape(1, -1),
        point_weight,
        residual_in,
        first_gain.reshape(1, -1),
        routes.T,
        route_score.T,
        expert_gate,
        expert_up,
        expert_down,
    )
    return (normed * second_gain).astype(bf16)


def solution(mesh):
    in_specs = (
        P("sp", "tp"),
        P("sp", "tp"),
        P(None, "tp"),
        P("tp"),
        P(),
        P(("sp", "tp"), None),
        P(),
        P(),
        P(("sp", "tp"), None),
        P(("sp", "tp"), None),
        P(("sp", "tp"), None, None),
        P(("sp", "tp"), None, None),
        P(("sp", "tp"), None, None),
    )
    out_specs = P(("sp", "tp"), None)
    return jax.shard_map(
        per_device, mesh=mesh, in_specs=in_specs, out_specs=out_specs, check_vma=False
    )
```

time: 131 us -> 83.2 us (0.64)
  matrix products: 28.1 us -> 0 us
  Pallas kernels: 67.9 us -> 80.9 us
  starting transfers between devices: 10.2 us -> 0 us
  blocking collectives: 8.47 us -> 0 us
  waiting for transfers between devices: 6.57 us -> 0 us
  local copies, waits for them, and re-layouts: 5.34 us -> 0.01 us
  other arithmetic: 4.08 us -> 2.1 us
    conv_general_dilated x1 -> x0, matrix products: 23.4 us -> none  [per_device(): lax.conv_general_dilated(glu[None], conv_taps[:, None, :], (1,), [(0, 0)]...]
    pallas_call x1, Pallas kernels: 67.9 us -> 80.9 us  [per_device(): pl.pallas_call(layer_kernel, out_shape=jax.ShapeDtypeStruct((rows, width)...]
    psum x1 -> x0, blocking collectives: 8.47 us -> none  [per_device(): lax.psum((jnp.sum(conv, axis=1), jnp.sum(conv * conv, axis=1)), 'tp')]
    ppermute x2 -> x0, starting transfers between devices: 6.5 us -> none  [from_behind(): return lax.ppermute(block, axis, route)]
    all_to_all x1 -> x0, waiting for transfers between devices: 5.41 us -> none  [per_device(): owned = lax.all_to_all(act, 'tp', split_axis=0, concat_axis=1, tiled=True)]
    dot_general x1 -> x0, matrix products: 4.75 us -> none  [per_device(): mix = jnp.dot(owned, point_weight, preferred_element_type=jnp.float32)]
    all_to_all x1 -> x0, starting transfers between devices: 3.65 us -> none  [per_device(): owned = lax.all_to_all(act, 'tp', split_axis=0, concat_axis=1, tiled=True)]
    unnamed x16 -> x2, local copies, waits for them, and re-layouts: 3.44 us -> 0.01 us
  transfers between devices with their start and end apart: 3 -> 0, of which waited for: 2 -> 0; matrix products, arithmetic and copies ran while one was open for 2% -> 0% of each run, Pallas kernels for 0% -> 0%
where the time goes in v2:
time: 83.2 us; the launch traced here: 83 us
  Pallas kernels  80.9 us (97%)
  other arithmetic  2.1 us (3%)
    pallas_call x1, Pallas kernels, per_device(): pl.pallas_call(layer_kernel, out_shape=jax.ShapeDtypeStruct((rows, width)...  80.9 us
    convert_element_type x1, other arithmetic, per_device(): return (normed * second_gain).astype(bf16)  2.1 us

profile of v2, /device:TPU:1, one launch (start us, length us, event | category | flops | bytes accessed | tf_op | source)
XLA Modules:
  0.0 83.0 jit_solution(1571676975161342406)
XLA Ops:
  0.0 0.0 copy-start
  0.0 80.9 %layer.1 = f32[128,2048]{1,0:T(8,128)} custom-call(bf16[512,512]{1,0:T(8,128)(2,1)} %value_hbm.1, bf16[512,512]{1,0:T(8,128)(2,1)} %gate_in_hbm.1, f32[31,512]{1,0:T(8,128)} %taps_ref.1, f32[1,512]{1,0:T(1,128)} %bitcast.5, bf16[2048,2048]{1,0:T(8,128)(2,1)} %point_hbm.1, bf16[128,2048]{1,0:T(8,128)(2,1)} %residual_hbm.1, f32[1,2048]{1,0:T(1,128)} %bitcast.4, ...), custom_call_target="tpu_custom_call" | custom-call | tf_op jit(solution)/shard_map/layer/pallas_call | solution.py:423
  80.9 0.0 copy-done
  80.9 2.1 %multiply_convert_fusion = bf16[128,2048]{1,0:T(8,128)(2,1)} fusion(f32[128,2048]{1,0:T(8,128)} %layer.1, f32[2048]{0:T(1024)S(1)} %copy-done), kind=kLoop, calls=%fused_computation | loop fusion | flops 524288 | bytes 1581056 | tf_op jit(solution)/shard_map/convert_element_type | solution.py:482
Async XLA Ops:
  0.0 80.9 %copy-start = (f32[2048]{0:T(1024)S(1)}, f32[2048]{0:T(1024)}, u32[]{:S(2)}) copy-start(f32[2048]{0:T(1024)} %param.20) | copy-start | bytes 24580

commit v3 on v2

--- a/solution.py
+++ b/solution.py
@@ -105,6 +105,7 @@
     recv_sem,
     back_send_sem,
     back_recv_sem,
+    word,
 ):
     inputs = [
         pltpu.make_async_copy(value_hbm, value, in_sem.at[0]),
@@ -117,15 +118,23 @@
         pltpu.make_async_copy(up_hbm.at[0], up_w, w_sem.at[3]),
         pltpu.make_async_copy(down_hbm.at[0], down_w, w_sem.at[4]),
     ]
-    for copy in inputs + weights:
+    for copy in inputs:
         copy.start()
     barrier = pltpu.get_barrier_semaphore()
 
-    def greet(k, carry):
-        pl.semaphore_signal(barrier, inc=1, device_id=partner(k, 1), device_id_type=MESH)
-        return carry
-
-    lax.fori_loop(1, PEERS, greet, 0)
+    sp, x = lax.axis_index("sp"), lax.axis_index("tp")
+    x_line = [partner(d, 1) for d in (1, 2, 3)]
+    y_line = [partner(4 * d, 1) for d in (1, 2, 3)]
+    z_line = [partner(16 * d, 1) for d in (1, 2, 3)]
+    twin = partner(HALF, 1)
+    beside = {"sp": (sp + 2 * (sp % 2) - 1 + 32) % 32, "tp": x}
+    met = x_line + y_line + z_line + [twin, beside]
+    for device in met:
+        pl.semaphore_signal(barrier, inc=1, device_id=device, device_id_type=MESH)
+
+    def spread_word(i, line):
+        for device in line:
+            pl.semaphore_signal(word.at[i], inc=1, device_id=device, device_id_type=MESH)
 
     rows, quarter = conv_own.shape
     width = quarter * QUARTERS
@@ -133,7 +142,6 @@
     lanes = glu.shape[3]
     chunks = quarter // lanes
     lead = glu.shape[2] - rows
-    sp, x = lax.axis_index("sp"), lax.axis_index("tp")
 
     def put_glu(block, values, start):
         for cc in range(chunks):
@@ -141,6 +149,8 @@
 
     for copy in inputs:
         copy.wait()
+    for copy in weights:
+        copy.start()
     for p in range(4):
         own = slice(p * rows, (p + 1) * rows)
         gated = value[own, :].astype(f32) * (1.0 / (1.0 + jnp.exp(-gate_in[own, :].astype(f32))))
@@ -148,17 +158,36 @@
         if p < 3:
             put_glu(p + 1, gated[rows - lead :], 0)
 
-    def convolve(p, into):
+    def convolve(p, into, first_row=0, end=rows):
         for cc in range(chunks):
             cols = slice(cc * lanes, (cc + 1) * lanes)
-            sum_ = jnp.zeros((rows, lanes), f32)
+            sum_ = jnp.zeros((end - first_row, lanes), f32)
             for j in range(taps_n):
-                sum_ = sum_ + taps_ref[j : j + 1, cols] * glu[p, cc, pl.ds(lead - taps_n + 1 + j, rows), :]
-            into[:, cols] = sum_.astype(bf16)
+                start = first_row + lead - taps_n + 1 + j
+                sum_ = sum_ + taps_ref[j : j + 1, cols] * glu[p, cc, pl.ds(start, end - first_row), :]
+            into[first_row:end, cols] = sum_.astype(bf16)
 
     order = order_of_blocks()
-    convolve(order[0], conv_send.at[0])
-    pl.semaphore_wait(barrier, PEERS - 1)
+
+    def conv_to(k, first_row=0, end=rows):
+        return pltpu.make_async_remote_copy(
+            src_ref=conv_send.at[k, pl.ds(first_row, end - first_row)],
+            dst_ref=conv_recv.at[(x - order[k] + 4) % 4 - 1, pl.ds(first_row, end - first_row)],
+            send_sem=conv_sem.at[0],
+            recv_sem=conv_sem.at[1],
+            device_id={"sp": sp, "tp": order[k]},
+            device_id_type=MESH,
+        )
+
+    def gain_to(d):
+        return pltpu.make_async_remote_copy(
+            src_ref=channel_gain_ref,
+            dst_ref=gains.at[3 - d],
+            send_sem=gain_sem.at[0],
+            recv_sem=gain_sem.at[1],
+            device_id={"sp": sp, "tp": (x + d) % 4},
+            device_id_type=MESH,
+        )
 
     total_rows = value.shape[0]
     behind = {"sp": (sp + 1) % 32, "tp": x}
@@ -173,39 +202,25 @@
         )
         for i, ref in enumerate((value, gate_in))
     ]
+    convolve(order[0], conv_send.at[0])
+    pl.semaphore_wait(barrier, len(met))
     for copy in rims:
         copy.start()
-
-    def conv_to(k):
-        return pltpu.make_async_remote_copy(
-            src_ref=conv_send.at[k],
-            dst_ref=conv_recv.at[(x - order[k] + 4) % 4 - 1],
-            send_sem=conv_sem.at[0],
-            recv_sem=conv_sem.at[1],
-            device_id={"sp": sp, "tp": order[k]},
-            device_id_type=MESH,
-        )
-
-    def gain_to(d):
-        return pltpu.make_async_remote_copy(
-            src_ref=channel_gain_ref,
-            dst_ref=gains.at[3 - d],
-            send_sem=gain_sem.at[0],
-            recv_sem=gain_sem.at[1],
-            device_id={"sp": sp, "tp": (x + d) % 4},
-            device_id_type=MESH,
-        )
-
     conv_to(0).start()
+    convolve(order[1], conv_send.at[1])
+    conv_to(1).start()
+    convolve(order[2], conv_send.at[2], lead, rows)
+    conv_to(2, lead, rows).start()
     for d in range(1, 4):
         gain_to(d).start()
-    convolve(order[1], conv_send.at[1])
-    conv_to(1).start()
+    spread_word(0, y_line)
     pltpu.make_async_copy(rim, rim, rim_sem.at[1]).wait()
     gated = rim[0].astype(f32) * (1.0 / (1.0 + jnp.exp(-rim[1].astype(f32))))
     put_glu(0, jnp.where(sp > 0, gated, jnp.zeros_like(gated)), 0)
-    convolve(order[2], conv_send.at[2])
-    conv_to(2).start()
+    convolve(order[2], conv_send.at[2], 0, lead)
+    conv_to(2, 0, lead).start()
+    pl.semaphore_wait(word.at[0], 3)
+    spread_word(1, z_line)
     convolve(order[3], conv_own)
 
     row = [routes_ref[k : k + 1, :] for k in range(2)]
@@ -232,7 +247,10 @@
         pick[pl.ds(pl.multiple_of(b * rows, rows), rows)] = (ids == key).astype(f32).astype(bf16)
         return carry
 
-    lax.fori_loop(0, 2 * QUARTERS, choose, 0)
+    lax.fori_loop(0, QUARTERS, choose, 0)
+    pl.semaphore_wait(word.at[1], 3)
+    spread_word(2, [twin])
+    lax.fori_loop(QUARTERS, 2 * QUARTERS, choose, 0)
 
     pltpu.make_async_copy(conv_recv, conv_recv, conv_sem.at[1]).wait()
     pltpu.make_async_copy(gains, gains, gain_sem.at[1]).wait()
@@ -275,8 +293,7 @@
         send[pl.ds(pl.multiple_of(b * 32, 32), 32)] = picked.reshape(32, BLOCK, quarter)
         return carry
 
-    lax.fori_loop(0, PEERS * BLOCK // 512, fill, 0)
-    recv[0] = send[0]
+    pl.semaphore_wait(word.at[2], 1)
     def dispatch_to(n, h):
         return pltpu.make_async_remote_copy(
             src_ref=send.at[n],
@@ -305,8 +322,11 @@
         dispatch_to(HALF + (k * 37) % HALF, 1).start()
         return carry
 
+    lax.fori_loop(0, HALF * BLOCK // 512, fill, 0)
     lax.fori_loop(1, HALF, near, 0)
+    lax.fori_loop(HALF * BLOCK // 512, PEERS * BLOCK // 512, fill, 0)
     lax.fori_loop(0, HALF, far, 0)
+    recv[0] = send[0]
 
     i = lax.broadcasted_iota(jnp.int32, (256, 256), 0)
     j = lax.broadcasted_iota(jnp.int32, (256, 256), 1)
@@ -422,7 +442,7 @@
     dma = pltpu.SemaphoreType.DMA
     normed = pl.pallas_call(
         layer_kernel,
-        out_shape=jax.ShapeDtypeStruct((rows, width), f32),
+        out_shape=pltpu.VMEM((rows, width), f32),
         in_specs=[hbm, hbm, vmem, vmem, hbm, hbm, vmem, vmem, vmem, hbm, hbm, hbm],
         out_specs=vmem,
         scratch_shapes=[
@@ -460,6 +480,7 @@
             dma((2,)),
             dma,
             dma((2,)),
+            pltpu.SemaphoreType.REGULAR((3,)),
         ],
         compiler_params=pltpu.CompilerParams(
             collective_id=1, has_side_effects=True, vmem_limit_bytes=60 * 1024 * 1024

time: 83.2 us -> 73.5 us (0.88)
  the two profiles are of different devices: /device:TPU:1 before, /device:TPU:33 now
where the time goes in v3:
time: 73.5 us; the launch traced here: 73.4 us
  Pallas kernels  72.5 us (99%)
  other arithmetic  0.88 us (1%)
    pallas_call x1, Pallas kernels, per_device(): pl.pallas_call(layer_kernel, out_shape=pltpu.VMEM((rows, width), f32), in...  72.5 us

profile of v3, /device:TPU:33, one launch (start us, length us, event | category | flops | bytes accessed | tf_op | source)
XLA Modules:
  0.0 73.4 jit_solution(4649784948277471490)
XLA Ops:
  0.0 0.0 copy-start
  0.0 72.5 %layer.1 = f32[128,2048]{1,0:T(8,128)S(1)} custom-call(bf16[512,512]{1,0:T(8,128)(2,1)} %value_hbm.1, bf16[512,512]{1,0:T(8,128)(2,1)} %gate_in_hbm.1, f32[31,512]{1,0:T(8,128)} %taps_ref.1, f32[1,512]{1,0:T(1,128)} %bitcast.5, bf16[2048,2048]{1,0:T(8,128)(2,1)} %point_hbm.1, bf16[128,2048]{1,0:T(8,128)(2,1)} %residual_hbm.1, f32[1,2048]{1,0:T(1,128)} %bitcast.4, ...), custom_call_target="tpu_custom_call" | custom-call | tf_op jit(solution)/shard_map/layer/pallas_call | solution.py:443
  72.5 0.0 copy-done
  72.5 0.9 %multiply_convert_fusion = bf16[128,2048]{1,0:T(8,128)(2,1)} fusion(f32[128,2048]{1,0:T(8,128)S(1)} %layer.1, f32[2048]{0:T(1024)S(1)} %copy-done), kind=kLoop, calls=%fused_computation | loop fusion | flops 524288 | bytes 1581056 | tf_op jit(solution)/shard_map/convert_element_type | solution.py:503
Async XLA Ops:
  0.0 72.5 %copy-start = (f32[2048]{0:T(1024)S(1)}, f32[2048]{0:T(1024)}, u32[]{:S(2)}) copy-start(f32[2048]{0:T(1024)} %param.20) | copy-start | bytes 24580

commit v4 on v3

--- a/solution.py
+++ b/solution.py
@@ -14,6 +14,13 @@
 PEERS, SLOTS, QUARTERS = 128, 4, 4
 BLOCK = SLOTS * QUARTERS
 HALF = PEERS // 2
+PARTS = ((0, 32), (32, 32), (64, 32), (96, 32))
+
+
+def far_to_near(part):
+    first, count = part
+    hops = (0, 1, 2, 1)
+    return [n for n in (first + (k * 37) % count for k in range(count)) if n > 0]
 
 
 def place():
@@ -23,15 +30,19 @@
 
 def partner(n, sign):
     x, y, z, c = place()
-    dx, dy, dz, dc = n % 4, (n // 4) % 4, (n // 16) % 4, n // 64
-    px, py, pz, pc = (x + sign * dx + 4) % 4, (y + sign * dy + 4) % 4, (z + sign * dz + 4) % 4, (c + dc) % 2
+    dx, dy, dz, dc = n % 4, (n // 4) % 4, (n // 16) % 2 * 2 + (n // 32) % 2, n // 64
+    pc = (c + dc) % 2
+    way = 1 - 2 * c if sign > 0 else 2 * pc - 1
+    px, py, pz = (x + way * dx + 4) % 4, (y + way * dy + 4) % 4, (z + way * dz + 4) % 4
     return {"sp": (pz * 4 + py) * 2 + pc, "tp": px}
 
 
 def offset_of(e):
     x, y, z, c = place()
     ex, ec, ey, ez = e & 3, (e >> 2) & 1, (e >> 3) & 3, e >> 5
-    return ((ec - c) & 1) * 64 + ((ez - z) & 3) * 16 + ((ey - y) & 3) * 4 + ((ex - x) & 3)
+    way = 1 - 2 * c
+    dz = (way * (ez - z)) & 3
+    return ((ec - c) & 1) * 64 + (dz & 1) * 32 + (dz >> 1) * 16 + ((way * (ey - y)) & 3) * 4 + ((way * (ex - x)) & 3)
 
 
 def slot_rows(mine, other, earlier, axis):
@@ -48,29 +59,35 @@
     return jnp.sum(jnp.where(same, row, jnp.zeros_like(row)), axis=1, keepdims=True)
 
 
-def order_of_blocks():
-    x = lax.axis_index("tp")
-    table = ((2, 1, 3, 0), (3, 2, 0, 1), (3, 1, 0, 2), (1, 2, 0, 3))
-    return [
-        jnp.where(x == 0, table[0][k], jnp.where(x == 1, table[1][k], jnp.where(x == 2, table[2][k], table[3][k])))
-        for k in range(4)
-    ]
+def along(col):
+    n = col.shape[0]
+    same = lax.broadcasted_iota(jnp.int32, (n, n), 0) == lax.broadcasted_iota(jnp.int32, (n, n), 1)
+    return jnp.sum(jnp.where(same, col, jnp.zeros_like(col)), axis=0, keepdims=True)
 
 
 def layer_kernel(
     value_hbm,
     gate_in_hbm,
-    taps_ref,
-    channel_gain_ref,
+    taps_hbm,
+    channel_gain_hbm,
     point_hbm,
     residual_hbm,
-    first_gain_ref,
-    routes_ref,
-    score_ref,
+    first_gain_hbm,
+    second_gain_hbm,
+    routes_hbm,
+    score_hbm,
     gate_hbm,
     up_hbm,
     down_hbm,
     out_ref,
+    taps_ref,
+    channel_gain_ref,
+    first_gain_ref,
+    second_gain_ref,
+    routes_ref,
+    score_ref,
+    stat_send,
+    stat_recv,
     value,
     gate_in,
     rim,
@@ -97,8 +114,10 @@
     pick,
     total,
     in_sem,
+    small_sem,
     w_sem,
     rim_sem,
+    stat_sem,
     gain_sem,
     conv_sem,
     send_sem,
@@ -110,6 +129,19 @@
     inputs = [
         pltpu.make_async_copy(value_hbm, value, in_sem.at[0]),
         pltpu.make_async_copy(gate_in_hbm, gate_in, in_sem.at[1]),
+        pltpu.make_async_copy(taps_hbm, taps_ref, in_sem.at[2]),
+    ]
+    small = [
+        pltpu.make_async_copy(src, dst, small_sem.at[i])
+        for i, (src, dst) in enumerate(
+            (
+                (channel_gain_hbm, channel_gain_ref),
+                (routes_hbm, routes_ref),
+                (score_hbm, score_ref),
+                (first_gain_hbm, first_gain_ref),
+                (second_gain_hbm, second_gain_ref),
+            )
+        )
     ]
     weights = [
         pltpu.make_async_copy(point_hbm, point, w_sem.at[0]),
@@ -118,14 +150,14 @@
         pltpu.make_async_copy(up_hbm.at[0], up_w, w_sem.at[3]),
         pltpu.make_async_copy(down_hbm.at[0], down_w, w_sem.at[4]),
     ]
-    for copy in inputs:
+    for copy in inputs + small:
         copy.start()
     barrier = pltpu.get_barrier_semaphore()
 
     sp, x = lax.axis_index("sp"), lax.axis_index("tp")
     x_line = [partner(d, 1) for d in (1, 2, 3)]
     y_line = [partner(4 * d, 1) for d in (1, 2, 3)]
-    z_line = [partner(16 * d, 1) for d in (1, 2, 3)]
+    z_line = [partner(n, 1) for n in (16, 32, 48)]
     twin = partner(HALF, 1)
     beside = {"sp": (sp + 2 * (sp % 2) - 1 + 32) % 32, "tp": x}
     met = x_line + y_line + z_line + [twin, beside]
@@ -158,7 +190,8 @@
         if p < 3:
             put_glu(p + 1, gated[rows - lead :], 0)
 
-    def convolve(p, into, first_row=0, end=rows):
+    def convolve(p, into, first_row, end):
+        one = two = jnp.zeros((end - first_row, 1), f32)
         for cc in range(chunks):
             cols = slice(cc * lanes, (cc + 1) * lanes)
             sum_ = jnp.zeros((end - first_row, lanes), f32)
@@ -166,15 +199,29 @@
                 start = first_row + lead - taps_n + 1 + j
                 sum_ = sum_ + taps_ref[j : j + 1, cols] * glu[p, cc, pl.ds(start, end - first_row), :]
             into[first_row:end, cols] = sum_.astype(bf16)
-
-    order = order_of_blocks()
-
-    def conv_to(k, first_row=0, end=rows):
+            one = one + jnp.sum(sum_, axis=1, keepdims=True)
+            two = two + jnp.sum(sum_ * sum_, axis=1, keepdims=True)
+        return one, two
+
+    ahead = (2, 1, 3)
+    order = [(x + d) % 4 for d in ahead] + [x]
+
+    def conv_to(k, first_row, end):
         return pltpu.make_async_remote_copy(
             src_ref=conv_send.at[k, pl.ds(first_row, end - first_row)],
-            dst_ref=conv_recv.at[(x - order[k] + 4) % 4 - 1, pl.ds(first_row, end - first_row)],
-            send_sem=conv_sem.at[0],
-            recv_sem=conv_sem.at[1],
+            dst_ref=conv_recv.at[3 - ahead[k], pl.ds(first_row, end - first_row)],
+            send_sem=conv_sem.at[3],
+            recv_sem=conv_sem.at[3 - ahead[k]],
+            device_id={"sp": sp, "tp": order[k]},
+            device_id_type=MESH,
+        )
+
+    def stat_to(k):
+        return pltpu.make_async_remote_copy(
+            src_ref=stat_send.at[k],
+            dst_ref=stat_recv.at[3 - ahead[k]],
+            send_sem=stat_sem.at[0],
+            recv_sem=stat_sem.at[1],
             device_id={"sp": sp, "tp": order[k]},
             device_id_type=MESH,
         )
@@ -202,26 +249,34 @@
         )
         for i, ref in enumerate((value, gate_in))
     ]
-    convolve(order[0], conv_send.at[0])
+    lower = [convolve(order[0], conv_send.at[0], lead, rows)]
     pl.semaphore_wait(barrier, len(met))
     for copy in rims:
         copy.start()
-    conv_to(0).start()
-    convolve(order[1], conv_send.at[1])
-    conv_to(1).start()
-    convolve(order[2], conv_send.at[2], lead, rows)
-    conv_to(2, lead, rows).start()
+    conv_to(0, lead, rows).start()
+    for k in (1, 2):
+        lower.append(convolve(order[k], conv_send.at[k], lead, rows))
+        conv_to(k, lead, rows).start()
+    small[0].wait()
     for d in range(1, 4):
         gain_to(d).start()
     spread_word(0, y_line)
+    lower.append(convolve(x, conv_own, lead, rows))
     pltpu.make_async_copy(rim, rim, rim_sem.at[1]).wait()
     gated = rim[0].astype(f32) * (1.0 / (1.0 + jnp.exp(-rim[1].astype(f32))))
     put_glu(0, jnp.where(sp > 0, gated, jnp.zeros_like(gated)), 0)
-    convolve(order[2], conv_send.at[2], 0, lead)
-    conv_to(2, 0, lead).start()
+    for k in range(3):
+        upper = convolve(order[k], conv_send.at[k], 0, lead)
+        for i in range(2):
+            stat_send[k, i : i + 1, :] = along(jnp.concatenate([upper[i], lower[k][i]], axis=0))
+        stat_to(k).start()
+        conv_to(k, 0, lead).start()
+    upper = convolve(x, conv_own, 0, lead)
+    sums = [along(jnp.concatenate([upper[i], lower[3][i]], axis=0)) for i in range(2)]
     pl.semaphore_wait(word.at[0], 3)
     spread_word(1, z_line)
-    convolve(order[3], conv_own)
+    for copy in small[1:]:
+        copy.wait()
 
     row = [routes_ref[k : k + 1, :] for k in range(2)]
     col = [across(r) for r in row]
@@ -252,32 +307,35 @@
     spread_word(2, [twin])
     lax.fori_loop(QUARTERS, 2 * QUARTERS, choose, 0)
 
-    pltpu.make_async_copy(conv_recv, conv_recv, conv_sem.at[1]).wait()
     pltpu.make_async_copy(gains, gains, gain_sem.at[1]).wait()
-    parts = [conv_own[...].astype(f32)] + [conv_recv[i].astype(f32) for i in range(3)]
-    middle = sum(jnp.sum(v, axis=1, keepdims=True) for v in parts) / width
-    spread = sum(jnp.sum(v * v, axis=1, keepdims=True) for v in parts) / width - middle * middle
-    scale = lax.rsqrt(spread + 1e-05)
-    for i in range(4):
-        gain = channel_gain_ref[...] if i == 0 else gains[i - 1]
-        act[i] = silu((parts[i] - middle) * scale * gain).astype(bf16)
+    pltpu.make_async_copy(stat_recv, stat_recv, stat_sem.at[1]).wait()
+    for k in range(3):
+        sums = [sums[i] + stat_recv[k, i : i + 1, :] for i in range(2)]
+    middle = sums[0] / width
+    spread = sums[1] / width - middle * middle
+    scale = across(lax.rsqrt(spread + 1e-05))
+    middle = across(middle)
     for copy in weights[:2]:
         copy.wait()
-
-    def mix(b, carry):
-        cols = pl.ds(pl.multiple_of(b * quarter, quarter), quarter)
-        sum_ = residual_scale * residual[:, cols].astype(f32)
-        for i in range(4):
-            block = (x + i) % 4
-            sum_ = sum_ + jnp.dot(
-                act[i],
+    for i in (0, 2, 3, 1):
+        if i > 0:
+            pltpu.make_async_copy(conv_recv.at[i - 1], conv_recv.at[i - 1], conv_sem.at[i - 1]).wait()
+        values = conv_own[...] if i == 0 else conv_recv[i - 1]
+        gain = channel_gain_ref[...] if i == 0 else gains[i - 1]
+        act[...] = silu((values.astype(f32) - middle) * scale * gain).astype(bf16)
+        block = (x + i) % 4
+
+        def mix(b, carry):
+            cols = pl.ds(pl.multiple_of(b * quarter, quarter), quarter)
+            part = jnp.dot(
+                act[...],
                 point[pl.ds(pl.multiple_of(block * quarter, quarter), quarter), cols],
                 preferred_element_type=f32,
             )
-        h1[b] = sum_
-        return carry
-
-    lax.fori_loop(0, QUARTERS, mix, 0)
+            h1[b] = (residual_scale * residual[:, cols].astype(f32) if i == 0 else h1[b]) + part
+            return carry
+
+        lax.fori_loop(0, QUARTERS, mix, 0)
     middle = sum(jnp.sum(h1[q], axis=1, keepdims=True) for q in range(QUARTERS)) / width
     centred = [h1[q] - middle for q in range(QUARTERS)]
     spread = sum(jnp.sum(v * v, axis=1, keepdims=True) for v in centred) / width
@@ -314,18 +372,11 @@
             device_id_type=MESH,
         )
 
-    def near(k, carry):
-        dispatch_to((k * 37) % HALF, 0).start()
-        return carry
-
-    def far(k, carry):
-        dispatch_to(HALF + (k * 37) % HALF, 1).start()
-        return carry
-
-    lax.fori_loop(0, HALF * BLOCK // 512, fill, 0)
-    lax.fori_loop(1, HALF, near, 0)
-    lax.fori_loop(HALF * BLOCK // 512, PEERS * BLOCK // 512, fill, 0)
-    lax.fori_loop(0, HALF, far, 0)
+    recv_group = 512 // BLOCK
+    for h, part in enumerate(PARTS):
+        lax.fori_loop(part[0] // recv_group, sum(part) // recv_group, fill, 0)
+        for n in far_to_near(part):
+            dispatch_to(n, h).start()
     recv[0] = send[0]
 
     i = lax.broadcasted_iota(jnp.int32, (256, 256), 0)
@@ -333,12 +384,12 @@
     to_flat = (((i // 4) % 16) * 16 + (i // 64) * 4 + i % 4 == j).astype(f32).astype(bf16)
     to_block = (((j // 4) % 16) * 16 + (j // 64) * 4 + j % 4 == i).astype(f32).astype(bf16)
 
-    for h in range(2):
-        start = h * HALF
-        own = 1 - h
-        landed = recv.at[pl.ds(start + own, HALF - own)]
+    for h, (start, count) in enumerate(PARTS):
+        own = 1 if h == 0 else 0
+        m = count * SLOTS
+        landed = recv.at[pl.ds(start + own, count - own)]
         pltpu.make_async_copy(landed, landed, recv_sem.at[h]).wait()
-        for g in range(4):
+        for g in range(count // 16):
             block = recv[pl.ds(start + g * 16, 16)].reshape(256, quarter)
             moved = jnp.dot(to_flat, block, preferred_element_type=f32).astype(bf16)
             for q in range(QUARTERS):
@@ -349,45 +400,31 @@
 
         def hide(b, carry):
             cols = pl.ds(pl.multiple_of(b * 256, 256), 256)
-            gate = jnp.dot(flat[...], gate_w[:, cols], preferred_element_type=f32)
-            upper = jnp.dot(flat[...], up_w[:, cols], preferred_element_type=f32)
-            hidden[:, cols] = (gate * jax.nn.sigmoid(gate) * upper).astype(bf16)
+            gate = jnp.dot(flat[:m], gate_w[:, cols], preferred_element_type=f32)
+            upper = jnp.dot(flat[:m], up_w[:, cols], preferred_element_type=f32)
+            hidden[:m, cols] = (silu(gate) * upper).astype(bf16)
             return carry
 
         lax.fori_loop(0, hidden.shape[1] // 256, hide, 0)
         for q in range(QUARTERS):
             cols = pl.ds(q * quarter, quarter)
-            result = jnp.dot(hidden[...], down_w[:, cols], preferred_element_type=f32).astype(bf16)
-            for g in range(4):
+            result = jnp.dot(hidden[:m], down_w[:, cols], preferred_element_type=f32).astype(bf16)
+            for g in range(count // 16):
                 answer[g, pl.ds(q * 64, 64), :] = result[g * 64 : (g + 1) * 64]
-        for g in range(4):
+        for g in range(count // 16):
             moved = jnp.dot(to_block, answer[g], preferred_element_type=f32).astype(bf16)
             back_send[pl.ds(start + g * 16, 16)] = moved.reshape(16, BLOCK, quarter)
         if h == 0:
             back_recv[0] = back_send[0]
-
-            def near_back(k, carry):
-                answer_to((k * 37) % HALF, 0).start()
-                return carry
-
-            lax.fori_loop(1, HALF, near_back, 0)
-        else:
-
-            def far_back(k, carry):
-                answer_to(HALF + (k * 37) % HALF, 1).start()
-                return carry
-
-            lax.fori_loop(0, HALF, far_back, 0)
-
-    for h in range(2):
-        start = h * HALF
-        own = 1 - h
-        landed = back_recv.at[pl.ds(start + own, HALF - own)]
+        for n in far_to_near((start, count)):
+            answer_to(n, h).start()
+
+    for h, (start, count) in enumerate(PARTS):
+        own = 1 if h == 0 else 0
+        landed = back_recv.at[pl.ds(start + own, count - own)]
         pltpu.make_async_copy(landed, landed, back_recv_sem.at[h]).wait()
-        block = back_recv[pl.ds(start, HALF)].reshape(HALF * BLOCK, quarter)
-        part = jnp.dot(
-            pick[:, pl.ds(start * BLOCK, HALF * BLOCK)], block, preferred_element_type=f32
-        )
+        block = back_recv[pl.ds(start, count)].reshape(count * BLOCK, quarter)
+        part = jnp.dot(pick[:, pl.ds(start * BLOCK, count * BLOCK)], block, preferred_element_type=f32)
         total[...] = part if h == 0 else total[...] + part
 
     share = [across(score_ref[k : k + 1, :] / (score_ref[0:1, :] + score_ref[1:2, :])) for k in range(2)]
@@ -402,12 +439,14 @@
     spread = sum(jnp.sum(m * m, axis=1, keepdims=True) for m in mixed) / width
     scale = lax.rsqrt(spread + 1e-05)
     for q in range(QUARTERS):
-        out_ref[:, q * quarter : (q + 1) * quarter] = mixed[q] * scale
+        cols = slice(q * quarter, (q + 1) * quarter)
+        out_ref[:, cols] = (mixed[q] * scale * second_gain_ref[:, cols]).astype(bf16)
 
     for copy in rims:
         copy.wait_send()
     for k in range(3):
-        conv_to(k).wait_send()
+        conv_to(k, 0, rows).wait_send()
+        stat_to(k).wait_send()
     for d in range(1, 4):
         gain_to(d).wait_send()
     sent = send.at[pl.ds(1, PEERS - 1)]
@@ -440,12 +479,20 @@
     hbm = pl.BlockSpec(memory_space=pl.ANY)
     blocks = pltpu.VMEM((PEERS, BLOCK, quarter), bf16)
     dma = pltpu.SemaphoreType.DMA
-    normed = pl.pallas_call(
+    return pl.pallas_call(
         layer_kernel,
-        out_shape=pltpu.VMEM((rows, width), f32),
-        in_specs=[hbm, hbm, vmem, vmem, hbm, hbm, vmem, vmem, vmem, hbm, hbm, hbm],
+        out_shape=pltpu.VMEM((rows, width), bf16),
+        in_specs=[hbm] * 13,
         out_specs=vmem,
         scratch_shapes=[
+            pltpu.VMEM(conv_taps.shape, f32),
+            pltpu.VMEM((1, quarter), f32),
+            pltpu.VMEM((1, width), f32),
+            pltpu.VMEM((1, width), f32),
+            pltpu.VMEM((2, rows), jnp.int32),
+            pltpu.VMEM((2, rows), f32),
+            pltpu.VMEM((3, 2, rows), f32),
+            pltpu.VMEM((3, 2, rows), f32),
             pltpu.VMEM((tokens, quarter), bf16),
             pltpu.VMEM((tokens, quarter), bf16),
             pltpu.VMEM((2, lead, quarter), bf16),
@@ -456,7 +503,7 @@
             pltpu.VMEM((3, 1, quarter), f32),
             pltpu.VMEM((width, width), bf16),
             pltpu.VMEM((rows, width), bf16),
-            pltpu.VMEM((4, rows, quarter), bf16),
+            pltpu.VMEM((rows, quarter), bf16),
             pltpu.VMEM((QUARTERS, rows, quarter), f32),
             pltpu.VMEM((QUARTERS * rows, quarter), bf16),
             pltpu.VMEM((width, inner), bf16),
@@ -471,15 +518,17 @@
             blocks,
             pltpu.VMEM((2 * QUARTERS * rows, PEERS * BLOCK), bf16),
             pltpu.VMEM((2 * QUARTERS * rows, quarter), f32),
-            dma((2,)),
+            dma((3,)),
+            dma((5,)),
             dma((5,)),
             dma((2,)),
             dma((2,)),
             dma((2,)),
+            dma((4,)),
             dma,
-            dma((2,)),
+            dma((4,)),
             dma,
-            dma((2,)),
+            dma((4,)),
             pltpu.SemaphoreType.REGULAR((3,)),
         ],
         compiler_params=pltpu.CompilerParams(
@@ -494,13 +543,13 @@
         point_weight,
         residual_in,
         first_gain.reshape(1, -1),
+        second_gain.reshape(1, -1),
         routes.T,
         route_score.T,
         expert_gate,
         expert_up,
         expert_down,
     )
-    return (normed * second_gain).astype(bf16)
 
 
 def solution(mesh):

time: 73.5 us -> 71.1 us (0.967)
  the two profiles are of different devices: /device:TPU:33 before, /device:TPU:1 now
where the time goes in v4:
time: 71.1 us; the launch traced here: 70.9 us
  Pallas kernels  70.1 us (99%)
  local copies, waits for them, and re-layouts  0.8 us (1%)
    pallas_call x1, Pallas kernels, per_device(): pl.pallas_call(layer_kernel, out_shape=pltpu.VMEM((rows, width), bf16), i...  70.1 us

profile of v4, /device:TPU:1, one launch (start us, length us, event | category | flops | bytes accessed | tf_op | source)
XLA Modules:
  0.0 70.9 jit_solution(1524605369501429658)
XLA Ops:
  0.0 70.1 %layer.1 = bf16[128,2048]{1,0:T(8,128)(2,1)S(1)} custom-call(bf16[512,512]{1,0:T(8,128)(2,1)} %value_hbm.1, bf16[512,512]{1,0:T(8,128)(2,1)} %gate_in_hbm.1, f32[31,512]{1,0:T(8,128)} %taps_hbm.1, f32[1,512]{1,0:T(1,128)} %bitcast.7, bf16[2048,2048]{1,0:T(8,128)(2,1)} %point_hbm.1, bf16[128,2048]{1,0:T(8,128)(2,1)} %residual_hbm.1, f32[1,2048]{1,0:T(1,128)} %bitcast.5, ...), custom_call_target="tpu_custom_call" | custom-call | tf_op jit(solution)/shard_map/layer/pallas_call | solution.py:482
  70.1 0.8 %copy.15 = bf16[128,2048]{1,0:T(8,128)(2,1)} copy(bf16[128,2048]{1,0:T(8,128)(2,1)S(1)} %layer.1) | data formatting | bytes 1048576

commit v5 on v4

--- a/solution.py
+++ b/solution.py
@@ -325,17 +325,14 @@
         act[...] = silu((values.astype(f32) - middle) * scale * gain).astype(bf16)
         block = (x + i) % 4
 
-        def mix(b, carry):
-            cols = pl.ds(pl.multiple_of(b * quarter, quarter), quarter)
+        for b in range(QUARTERS):
+            cols = slice(b * quarter, (b + 1) * quarter)
             part = jnp.dot(
                 act[...],
                 point[pl.ds(pl.multiple_of(block * quarter, quarter), quarter), cols],
                 preferred_element_type=f32,
             )
             h1[b] = (residual_scale * residual[:, cols].astype(f32) if i == 0 else h1[b]) + part
-            return carry
-
-        lax.fori_loop(0, QUARTERS, mix, 0)
     middle = sum(jnp.sum(h1[q], axis=1, keepdims=True) for q in range(QUARTERS)) / width
     centred = [h1[q] - middle for q in range(QUARTERS)]
     spread = sum(jnp.sum(v * v, axis=1, keepdims=True) for v in centred) / width

time: 71.1 us -> 68.4 us (0.962)
  Pallas kernels: 70.1 us -> 67.5 us
    pallas_call x1, Pallas kernels: 70.1 us -> 67.5 us  [per_device(): pl.pallas_call(layer_kernel, out_shape=pltpu.VMEM((rows, width), bf16), i...]
where the time goes in v5:
time: 68.4 us; the launch traced here: 68.3 us
  Pallas kernels  67.5 us (99%)
  local copies, waits for them, and re-layouts  0.8 us (1%)
    pallas_call x1, Pallas kernels, per_device(): pl.pallas_call(layer_kernel, out_shape=pltpu.VMEM((rows, width), bf16), i...  67.5 us

profile of v5, /device:TPU:1, one launch (start us, length us, event | category | flops | bytes accessed | tf_op | source)
XLA Modules:
  0.0 68.3 jit_solution(17912176711295148536)
XLA Ops:
  0.0 67.5 %layer.1 = bf16[128,2048]{1,0:T(8,128)(2,1)S(1)} custom-call(bf16[512,512]{1,0:T(8,128)(2,1)} %value_hbm.1, bf16[512,512]{1,0:T(8,128)(2,1)} %gate_in_hbm.1, f32[31,512]{1,0:T(8,128)} %taps_hbm.1, f32[1,512]{1,0:T(1,128)} %bitcast.7, bf16[2048,2048]{1,0:T(8,128)(2,1)} %point_hbm.1, bf16[128,2048]{1,0:T(8,128)(2,1)} %residual_hbm.1, f32[1,2048]{1,0:T(1,128)} %bitcast.5, ...), custom_call_target="tpu_custom_call" | custom-call | tf_op jit(solution)/shard_map/layer/pallas_call | solution.py:479
  67.5 0.8 %copy.15 = bf16[128,2048]{1,0:T(8,128)(2,1)} copy(bf16[128,2048]{1,0:T(8,128)(2,1)S(1)} %layer.1) | data formatting | bytes 1048576

commit v6 on v5

--- a/solution.py
+++ b/solution.py
@@ -203,7 +203,7 @@
             two = two + jnp.sum(sum_ * sum_, axis=1, keepdims=True)
         return one, two
 
-    ahead = (2, 1, 3)
+    ahead = (1, 3, 2)
     order = [(x + d) % 4 for d in ahead] + [x]
 
     def conv_to(k, first_row, end):
@@ -254,9 +254,9 @@
     for copy in rims:
         copy.start()
     conv_to(0, lead, rows).start()
-    for k in (1, 2):
-        lower.append(convolve(order[k], conv_send.at[k], lead, rows))
-        conv_to(k, lead, rows).start()
+    lower.append(convolve(order[1], conv_send.at[1], lead, rows))
+    conv_to(1, lead, rows).start()
+    lower.append(convolve(order[2], conv_send.at[2], lead, rows))
     small[0].wait()
     for d in range(1, 4):
         gain_to(d).start()
@@ -270,6 +270,8 @@
         for i in range(2):
             stat_send[k, i : i + 1, :] = along(jnp.concatenate([upper[i], lower[k][i]], axis=0))
         stat_to(k).start()
+    conv_to(2, 0, rows).start()
+    for k in range(2):
         conv_to(k, 0, lead).start()
     upper = convolve(x, conv_own, 0, lead)
     sums = [along(jnp.concatenate([upper[i], lower[3][i]], axis=0)) for i in range(2)]
@@ -317,7 +319,7 @@
     middle = across(middle)
     for copy in weights[:2]:
         copy.wait()
-    for i in (0, 2, 3, 1):
+    for i in (0, 3, 1, 2):
         if i > 0:
             pltpu.make_async_copy(conv_recv.at[i - 1], conv_recv.at[i - 1], conv_sem.at[i - 1]).wait()
         values = conv_own[...] if i == 0 else conv_recv[i - 1]

time: 68.4 us -> 68.3 us (level)
  no operation moved by 1% of the time
where the time goes in v6:
time: 68.3 us; the launch traced here: 68.1 us
  Pallas kernels  67.3 us (99%)
  local copies, waits for them, and re-layouts  0.8 us (1%)
    pallas_call x1, Pallas kernels, per_device(): pl.pallas_call(layer_kernel, out_shape=pltpu.VMEM((rows, width), bf16), i...  67.3 us

profile of v6, /device:TPU:1, one launch (start us, length us, event | category | flops | bytes accessed | tf_op | source)
XLA Modules:
  0.0 68.1 jit_solution(6805711577933984281)
XLA Ops:
  0.0 67.3 %layer.1 = bf16[128,2048]{1,0:T(8,128)(2,1)S(1)} custom-call(bf16[512,512]{1,0:T(8,128)(2,1)} %value_hbm.1, bf16[512,512]{1,0:T(8,128)(2,1)} %gate_in_hbm.1, f32[31,512]{1,0:T(8,128)} %taps_hbm.1, f32[1,512]{1,0:T(1,128)} %bitcast.7, bf16[2048,2048]{1,0:T(8,128)(2,1)} %point_hbm.1, bf16[128,2048]{1,0:T(8,128)(2,1)} %residual_hbm.1, f32[1,2048]{1,0:T(1,128)} %bitcast.5, ...), custom_call_target="tpu_custom_call" | custom-call | tf_op jit(solution)/shard_map/layer/pallas_call | solution.py:481
  67.4 0.8 %copy.15 = bf16[128,2048]{1,0:T(8,128)(2,1)} copy(bf16[128,2048]{1,0:T(8,128)(2,1)S(1)} %layer.1) | data formatting | bytes 1048576
